TPU v7x, 32 devices: a whole 2x2x4 slice. The times are simulated.
32 devices in a mesh: rep: 2 (over y), fs: 4 (over z), tp: 4 (over x, core).
Axes of the slice: x: 2, y: 2, z: 4, core: 2. Of those that a mesh axis runs over, the one named last changes fastest.
Arguments:
- tokens: bfloat16 [8, 512, 2048], P(('rep', 'fs')), may hold values from -6 to 6
- first_gain: float32 [2048], replicated, may hold values from 0.1 to 1.9
- in_matrix: float32 [2048, 2048], P('fs', 'tp'), may hold values from -0.125 to 0.125
- in_scale: float32 [2048], P('tp'), may hold values from 0.5 to 2
- conv_taps: float32 [4, 2048], P(None, 'tp'), may hold values from -3 to 3
- decay_rate: float32 [2, 2048], P(None, 'tp'), may hold values from 0 to 1, as said below
- recall_maps: float32 [2, 8, 256, 256], P(None, 'tp'), may hold values from -0.375 to 0.375
- admit_maps: float32 [2, 8, 256, 256], P(None, 'tp'), may hold values from -0.375 to 0.375
- out_matrix: float32 [2048, 2048], P('fs', 'tp'), may hold values from -0.125 to 0.125
- out_scale: float32 [2048], P('fs'), may hold values from 0.5 to 2
- second_gain: float32 [2048], replicated, may hold values from 0.1 to 1.9
- up_matrix: float32 [2048, 4096], P('fs', 'tp'), may hold values from -0.125 to 0.125
- up_scale: float32 [4096], P('tp'), may hold values from 0.5 to 2
- down_matrix: float32 [2048, 4096], P('fs', 'tp'), may hold values from -0.09375 to 0.09375
- down_scale: float32 [2048], P('fs'), may hold values from 0.5 to 2
Outputs:
- layer_out: bfloat16 [8, 512, 2048], P(('rep', 'fs'))
Inputs may be any that keep to these rules, and one draw needn't show every extreme that they name: `decay_rate`: positive per-step decay rates.
All inputs are finite; a program needn't handle non-finite values.
Results may differ from a plain program's by a relative error of at most 0.024.
Values may be sent and summed in bfloat16 or wider, within the bound.
A program may use at most 64 MiB of HBM per device.

v0:
```python
import functools
import jax
import jax.numpy as jnp
from jax import lax
from jax.experimental import pallas as pl
from jax.experimental.pallas import tpu as pltpu
from jax.sharding import PartitionSpec as P

EPSILON = 1e-06
RATE_GAIN = 8.0
LANES = 128
SEGMENTS = 8
PAD = 8


def normalize(stream, gain):
    return stream * lax.rsqrt(jnp.mean(stream * stream, axis=-1, keepdims=True) + EPSILON) * gain


def one_minus_exp(y):
    series = 1.0 + y * (1.0 / 6.0)
    for k in (5.0, 4.0, 3.0, 2.0):
        series = 1.0 + y * (1.0 / k) * series
    return jnp.where(y > -0.25, -y * series, 1.0 - jnp.exp(y))


def sigmoid(x):
    return 0.5 * jnp.tanh(0.5 * x) + 0.5


def gate_part(padded, taps_ref, rate_ref, recall_ref, admit_ref, decay, drive, length):
    directions, groups, block, _ = recall_ref.shape
    taps = taps_ref.shape[0]
    rows = length // SEGMENTS

    def tile_step(tile, _):
        base = pl.multiple_of(tile * rows, rows)
        conv = jnp.zeros((rows, padded.shape[1]), jnp.float32)
        window = padded[pl.ds(base, rows + 2 * PAD), :]
        for k in range(taps):
            first = PAD - taps // 2 + k
            conv = conv + taps_ref[k : k + 1, :] * window[first : first + rows, :]
        narrow = conv.astype(jnp.bfloat16)
        for g in range(groups):
            values = conv[:, g * block : (g + 1) * block]
            left = narrow[:, g * block : (g + 1) * block]
            for d in range(directions):
                recall = sigmoid(jnp.dot(left, recall_ref[d, g].astype(jnp.bfloat16), preferred_element_type=jnp.float32))
                admit = sigmoid(jnp.dot(left, admit_ref[d, g].astype(jnp.bfloat16), preferred_element_type=jnp.float32))
                log_decay = recall * (-RATE_GAIN * rate_ref[d : d + 1, g * block : (g + 1) * block])
                a = jnp.exp(log_decay)
                b = jnp.sqrt(one_minus_exp(2.0 * log_decay)) * admit * values
                for c in range(block // LANES):
                    where = g * (block // LANES) + c
                    decay[d, where, pl.ds(base, rows), :] = a[:, c * LANES : (c + 1) * LANES]
                    drive[d, where, pl.ds(base, rows), :] = b[:, c * LANES : (c + 1) * LANES]
        return 0

    lax.fori_loop(0, SEGMENTS, tile_step, 0)


def scan_part(decay, drive, prefix, mixed_ref, length):
    directions, chunks = decay.shape[:2]
    steps = length // SEGMENTS
    lanes = [(d, c) for d in range(directions) for c in range(chunks)]

    def scan_step(s, carried):
        out = []
        for (d, c), (state, product) in zip(lanes, carried):
            at = s if d == 0 else steps - 1 - s
            a = decay[d, c, pl.ds(at, SEGMENTS, stride=steps), :]
            b = drive[d, c, pl.ds(at, SEGMENTS, stride=steps), :]
            state = a * state + b
            product = a * product
            drive[d, c, pl.ds(at, SEGMENTS, stride=steps), :] = state
            prefix[d, c, pl.ds(at, SEGMENTS, stride=steps), :] = product
            out.append((state, product))
        return tuple(out)

    start = tuple((jnp.zeros((SEGMENTS, LANES), jnp.float32), jnp.ones((SEGMENTS, LANES), jnp.float32)) for _ in lanes)
    ends = lax.fori_loop(0, steps, scan_step, start, unroll=4)
    ends = dict(zip(lanes, ends))

    for c in range(chunks):
        carries = []
        for d in range(directions):
            state, product = ends[(d, c)]
            order = range(SEGMENTS) if d == 0 else range(SEGMENTS - 1, -1, -1)
            carry = jnp.zeros((1, LANES), jnp.float32)
            entering = {}
            for k in order:
                entering[k] = carry
                carry = product[k : k + 1, :] * carry + state[k : k + 1, :]
            carries.append(entering)
        for k in range(SEGMENTS):
            span = pl.ds(k * steps, steps)
            total = drive[0, c, span, :] + prefix[0, c, span, :] * carries[0][k]
            total = total + (drive[1, c, span, :] + prefix[1, c, span, :] * carries[1][k])
            mixed_ref[span, c * LANES : (c + 1) * LANES] = total.astype(jnp.bfloat16)


def recurrence_kernel(before_ref, taps_ref, rate_ref, recall_ref, admit_ref, mixed_ref, padded, decay, drive, prefix):
    length, width = before_ref.shape
    edge = jnp.zeros((PAD, width), jnp.float32)
    padded[pl.ds(0, PAD), :] = edge
    padded[pl.ds(PAD + length, PAD), :] = edge
    padded[pl.ds(PAD, length), :] = before_ref[...].astype(jnp.float32)
    gate_part(padded, taps_ref, rate_ref, recall_ref, admit_ref, decay, drive, length)
    scan_part(decay, drive, prefix, mixed_ref, length)


def recurrence(before, taps, rates, recall_maps, admit_maps):
    length, width = before.shape
    directions = rates.shape[0]
    chunks = width // LANES
    plane = pltpu.VMEM((directions, chunks, length, LANES), jnp.float32)
    return pl.pallas_call(
        recurrence_kernel,
        out_shape=jax.ShapeDtypeStruct((length, width), jnp.bfloat16),
        in_specs=[pl.BlockSpec(memory_space=pltpu.VMEM)] * 5,
        out_specs=pl.BlockSpec(memory_space=pltpu.VMEM),
        scratch_shapes=[pltpu.VMEM((length + 2 * PAD, width), jnp.float32), plane, plane, plane],
        compiler_params=pltpu.CompilerParams(vmem_limit_bytes=24 * 2**20),
        cost_estimate=pl.CostEstimate(flops=16 * length * width * 256, bytes_accessed=8 * 2**20, transcendentals=8 * length * width),
        name="recurrence",
    )(before, taps, rates, recall_maps, admit_maps)


def contract_last(left, right):
    return lax.dot_general(
        left, right, (((1,), (1,)), ((), ())), preferred_element_type=jnp.float32
    )


def gather(shard):
    copies = lax.axis_size("rep")
    if shard.shape[0] % (16 * copies):
        return lax.all_gather(shard.astype(jnp.bfloat16), "fs", axis=0, tiled=True)
    rows = shard.shape[0] // copies
    part = lax.dynamic_slice_in_dim(shard, lax.axis_index("rep") * rows, rows, 0)
    return lax.all_gather(part.astype(jnp.bfloat16), ("fs", "rep"), axis=0, tiled=True)


def body(
    tokens,
    first_gain,
    in_matrix,
    in_scale,
    conv_taps,
    decay_rate,
    recall_maps,
    admit_maps,
    out_matrix,
    out_scale,
    second_gain,
    up_matrix,
    up_scale,
    down_matrix,
    down_scale,
):
    stream = tokens.reshape(tokens.shape[1], tokens.shape[2]).astype(jnp.float32)
    factors = lax.all_gather(
        jnp.stack([out_scale, down_scale]).astype(jnp.bfloat16), "fs", axis=1, tiled=True
    )
    in_cols = gather(in_matrix)
    normed = normalize(stream, first_gain).astype(jnp.bfloat16)
    before = (
        jnp.dot(normed, in_cols, preferred_element_type=jnp.float32) * in_scale.astype(jnp.bfloat16)
    ).astype(jnp.bfloat16)
    mixed = recurrence(before, conv_taps, decay_rate, recall_maps, admit_maps)
    partial_value = contract_last(mixed, gather(out_matrix))
    middle = stream + factors[0] * lax.psum(partial_value.astype(jnp.bfloat16), "tp").astype(
        jnp.float32
    )
    second_normed = normalize(middle, second_gain).astype(jnp.bfloat16)
    raised = jnp.dot(second_normed, gather(up_matrix), preferred_element_type=jnp.float32)
    active = jnp.square(jax.nn.relu(raised * up_scale.astype(jnp.bfloat16))).astype(jnp.bfloat16)
    lowered = contract_last(active, gather(down_matrix))
    result = (
        middle + factors[1] * lax.psum(lowered.astype(jnp.bfloat16), "tp").astype(jnp.float32)
    ).astype(jnp.bfloat16)
    return result.reshape(tokens.shape)

MESH = pl.DeviceIdType.MESH


def layer_kernel(
    names, tokens_ref, first_ref, in_ref, in_scale_ref, taps_ref, rate_ref, recall_ref, admit_ref,
    out_ref, second_ref, up_ref, up_scale_ref, down_ref, scales_ref,
    result_ref,
    in_all, out_all, up_all, down_all, scales_all, normed, padded, decay, drive, prefix, mixed, active,
    first_parts, first_sums, second_parts, second_sums, middle, send, recv,
):
    replica, place, rank = (lax.axis_index(name) for name in names)
    rep_name, fs_name, tp_name = names
    fs, tp = 4, 4
    length, model = tokens_ref.shape
    rows = length // tp
    block = model // fs
    right, left, across = (lax.rem(place + k, fs) for k in (1, 3, 2))
    mate = 1 - replica
    near = rank + 1 - 2 * lax.rem(rank, 2)
    far = lax.rem(rank + 2, tp)
    count = [0]

    def copy(src, dst, axis, peer):
        index = count[0]
        count[0] += 1
        return pltpu.make_async_remote_copy(
            src_ref=src, dst_ref=dst, send_sem=send.at[index], recv_sem=recv.at[index],
            device_id={axis: peer}, device_id_type=MESH,
        )

    started = []

    def start(*copies):
        for one in copies:
            one.start()
            started.append(one)

    class Gather:
        def __init__(self, whole):
            def view(owner, offset, size):
                return whole.at[pl.ds(pl.multiple_of(owner * block + replica * half + offset, quarter), size), :]

            half, quarter = block // 2, block // 4
            own = view(place, 0, half)
            from_left, from_right = view(left, 0, half), view(right, 0, half)
            self.to_right = copy(own, own, fs_name, right)
            self.to_left = copy(own, own, fs_name, left)
            low, high = view(left, 0, quarter), view(right, quarter, quarter)
            self.on_right = copy(low, low, fs_name, right)
            self.on_left = copy(high, high, fs_name, left)
            opposite = view(across, 0, half)
            self.swaps = [copy(part, part, rep_name, mate) for part in (from_left, from_right, opposite)]

        def first(self):
            start(self.to_right, self.to_left)

        def second(self):
            self.to_right.wait_recv()
            start(self.on_right, self.swaps[0])
            self.to_left.wait_recv()
            start(self.on_left, self.swaps[1])

        def third(self):
            self.on_right.wait_recv()
            self.on_left.wait_recv()
            start(self.swaps[2])

        def finish(self):
            for swap in self.swaps:
                swap.wait_recv()

    barrier = pltpu.get_barrier_semaphore()
    greeted = [(rep_name, mate), (fs_name, right), (fs_name, left), (fs_name, across)]
    greeted += [(tp_name, lax.rem(rank + k, tp)) for k in range(1, tp)]
    for axis, peer in greeted:
        pl.semaphore_signal(barrier, inc=1, device_id={axis: peer}, device_id_type=MESH)

    own_rows = pl.ds(pl.multiple_of(place * block, block), block)
    for shard, whole in ((in_ref, in_all), (out_ref, out_all), (up_ref, up_all), (down_ref, down_all)):
        whole[own_rows, :] = shard[...].astype(jnp.bfloat16)
    scales_all[place] = scales_ref[...]
    pl.semaphore_wait(barrier, len(greeted))

    g_in, g_out, g_up, g_down = (Gather(whole) for whole in (in_all, out_all, up_all, down_all))
    g_in.first()
    scale_copies = [
        copy(scales_ref, scales_all.at[place], fs_name, lax.rem(place + k, fs)) for k in range(1, fs)
    ]
    start(*scale_copies)
    g_out.first()

    tile = 64

    def norm_step(i, _):
        at = pl.ds(pl.multiple_of(i * tile, tile), tile)
        normed[at, :] = normalize(tokens_ref[at, :].astype(jnp.float32), first_ref[...]).astype(jnp.bfloat16)
        return 0

    lax.fori_loop(0, length // tile, norm_step, 0)

    g_in.second()
    g_in.third()
    g_out.second()
    g_up.first()
    g_in.finish()

    edge = jnp.zeros((PAD, padded.shape[1]), jnp.float32)
    padded[pl.ds(0, PAD), :] = edge
    padded[pl.ds(PAD + length, PAD), :] = edge
    wide = 256

    def in_step(i, _):
        at = pl.ds(pl.multiple_of(i * wide, wide), wide)
        product = jnp.dot(normed[...], in_all[:, at], preferred_element_type=jnp.float32)
        product = product * in_scale_ref[:, at].astype(jnp.bfloat16).astype(jnp.float32)
        padded[pl.ds(PAD, length), at] = product.astype(jnp.bfloat16).astype(jnp.float32)
        return 0

    lax.fori_loop(0, in_all.shape[1] // wide, in_step, 0)
    g_out.third()
    gate_part(padded, taps_ref, rate_ref, recall_ref, admit_ref, decay, drive, length)
    g_up.second()
    g_down.first()
    scan_part(decay, drive, prefix, mixed, length)
    g_up.third()
    g_out.finish()
    for one in scale_copies:
        one.wait_recv()

    def project(values, whole, parts, sums, between):
        hops = []

        def send_block(j):
            hop = []
            for k in range(1, tp):
                peer = lax.rem(rank + k, tp)
                hop.append(copy(parts.at[j, pl.ds(pl.multiple_of(peer * rows, rows), rows), :], sums.at[k - 1, j], tp_name, peer))
            start(*hop)
            hops.append(hop)

        for j in range(fs):
            def step(i, _):
                at = pl.ds(pl.multiple_of(i * wide, wide), wide)
                matrix = whole[pl.ds(pl.multiple_of(j * block + i * wide, wide), wide), :]
                parts[j, :, at] = contract_last(values[...], matrix).astype(jnp.bfloat16)
                return 0

            lax.fori_loop(0, block // wide, step, 0)
            if j:
                send_block(j - 1)
            between(j)
        send_block(fs - 1)
        return hops

    own_quarter = pl.ds(pl.multiple_of(rank * rows, rows), rows)

    def summed(parts, sums, hops, j):
        for hop in hops[j]:
            hop.wait_recv()
        total = parts[j, own_quarter, :].astype(jnp.float32)
        for k in range(tp - 1):
            total = total + sums[k, j].astype(jnp.float32)
        return total

    def factor(j, which):
        return scales_all[j, which : which + 1, :].astype(jnp.bfloat16).astype(jnp.float32)

    def advance(j):
        if j == 1:
            g_down.second()

    hops = project(mixed, out_all, first_parts, first_sums, advance)
    squares = jnp.zeros((rows, 1), jnp.float32)
    for j in range(fs):
        columns = slice(j * block, (j + 1) * block)
        value = tokens_ref[own_quarter, columns].astype(jnp.float32) + factor(j, 0) * summed(first_parts, first_sums, hops, j)
        middle[:, columns] = value
        squares = squares + jnp.sum(value * value, axis=1, keepdims=True)
    inverse = lax.rsqrt(squares * (1.0 / model) + EPSILON)
    normed[own_quarter, :] = (middle[...] * inverse * second_ref[...]).astype(jnp.bfloat16)

    def spread(ref, columns):
        own = ref.at[own_quarter, columns]
        theirs = ref.at[pl.ds(pl.multiple_of(far * rows, rows), rows), columns]
        return copy(own, own, tp_name, far), copy(own, own, tp_name, near), copy(theirs, theirs, tp_name, near)

    whole_width = pl.ds(0, model)
    to_far, to_near, onward = spread(normed, whole_width)
    g_up.finish()
    start(to_far, to_near)
    g_down.third()
    to_far.wait_recv()
    start(onward)
    to_near.wait_recv()
    onward.wait_recv()

    def up_step(i, _):
        at = pl.ds(pl.multiple_of(i * wide, wide), wide)
        raised = jnp.dot(normed[...], up_all[:, at], preferred_element_type=jnp.float32)
        raised = raised * up_scale_ref[:, at].astype(jnp.bfloat16).astype(jnp.float32)
        active[:, at] = jnp.square(jnp.maximum(raised, 0.0)).astype(jnp.bfloat16)
        return 0

    lax.fori_loop(0, up_all.shape[1] // wide, up_step, 0)
    g_down.finish()
    hops = project(active, down_all, second_parts, second_sums, lambda j: None)
    spreads = []
    for j in range(fs):
        columns = slice(j * block, (j + 1) * block)
        value = middle[:, columns] + factor(j, 1) * summed(second_parts, second_sums, hops, j)
        result_ref[own_quarter, columns] = value.astype(jnp.bfloat16)
        spreads.append(spread(result_ref, pl.ds(j * block, block)))
        start(*spreads[j][:2])
        if j:
            spreads[j - 1][0].wait_recv()
            start(spreads[j - 1][2])
    spreads[-1][0].wait_recv()
    start(spreads[-1][2])
    for _, to_near, onward in spreads:
        to_near.wait_recv()
        onward.wait_recv()
    for one in started:
        one.wait_send()


def fused_body(
    tokens, first_gain, in_matrix, in_scale, conv_taps, decay_rate, recall_maps, admit_maps,
    out_matrix, out_scale, second_gain, up_matrix, up_scale, down_matrix, down_scale,
):
    length, model = tokens.shape[1:]
    width, hidden = in_matrix.shape[1], up_matrix.shape[1]
    fs, tp = lax.axis_size("fs"), lax.axis_size("tp")
    rows, block = length // tp, model // fs
    directions = decay_rate.shape[0]
    plane = pltpu.VMEM((directions, width // LANES, length, LANES), jnp.float32)
    parts = pltpu.VMEM((fs, length, block), jnp.bfloat16)
    sums = pltpu.VMEM((tp - 1, fs, rows, block), jnp.bfloat16)
    copies = 4 * 7 + 3 + 2 * 12 + 3 + 12
    result = pl.pallas_call(
        functools.partial(layer_kernel, ("rep", "fs", "tp")),
        out_shape=jax.ShapeDtypeStruct((length, model), jnp.bfloat16),
        in_specs=[pl.BlockSpec(memory_space=pltpu.VMEM)] * 14,
        out_specs=pl.BlockSpec(memory_space=pltpu.VMEM),
        scratch_shapes=[
            pltpu.VMEM((model, width), jnp.bfloat16),
            pltpu.VMEM((model, width), jnp.bfloat16),
            pltpu.VMEM((model, hidden), jnp.bfloat16),
            pltpu.VMEM((model, hidden), jnp.bfloat16),
            pltpu.VMEM((fs, 2, block), jnp.float32),
            pltpu.VMEM((length, model), jnp.bfloat16),
            pltpu.VMEM((length + 2 * PAD, width), jnp.float32),
            plane, plane, plane,
            pltpu.VMEM((length, width), jnp.bfloat16),
            pltpu.VMEM((length, hidden), jnp.bfloat16),
            parts, sums, parts, sums,
            pltpu.VMEM((rows, model), jnp.float32),
            pltpu.SemaphoreType.DMA((copies,)),
            pltpu.SemaphoreType.DMA((copies,)),
        ],
        compiler_params=pltpu.CompilerParams(
            collective_id=0, has_side_effects=True, vmem_limit_bytes=61 * 2**20
        ),
        name="layer",
    )(
        tokens.reshape(length, model), first_gain[None], in_matrix, in_scale[None], conv_taps, decay_rate,
        recall_maps, admit_maps, out_matrix, second_gain[None], up_matrix, up_scale[None], down_matrix,
        jnp.stack([out_scale, down_scale]),
    )
    return result.reshape(tokens.shape)


def solution(mesh):
    placed = (
        P(("rep", "fs"), None, None),
        P(),
        P("fs", "tp"),
        P("tp"),
        P(None, "tp"),
        P(None, "tp"),
        P(None, "tp", None, None),
        P(None, "tp", None, None),
        P("fs", "tp"),
        P("fs"),
        P(),
        P("fs", "tp"),
        P("tp"),
        P("fs", "tp"),
        P("fs"),
    )
    small = (mesh.shape["rep"], mesh.shape["fs"], mesh.shape["tp"]) == (2, 4, 4)
    return jax.shard_map(
        fused_body if small else body, mesh=mesh, in_specs=placed, out_specs=P(("rep", "fs"), None, None), check_vma=False
    )
```

profile of v0, /device:TPU:0, one launch (start us, length us, event | category | flops | bytes accessed | tf_op | source)
XLA Modules:
  0.0 183.2 jit_solution(7191453015904008897)
XLA Ops:
  0.0 1.3 pad_maximum_fusion.scales_ref
  1.3 178.7 %layer.1 = bf16[512,2048]{1,0:T(8,128)(2,1)} custom-call(bf16[512,2048]{1,0:T(8,128)(2,1)} %bitcast.9, f32[1,2048]{1,0:T(1,128)} %bitcast.10, f32[512,512]{1,0:T(8,128)} %in_ref.1, f32[1,512]{1,0:T(1,128)} %bitcast.13, f32[4,512]{1,0:T(4,128)} %taps_ref.1, f32[2,512]{1,0:T(2,128)} %rate_ref.1, f32[2,2,256,256]{3,2,1,0:T(8,128)} %recall_ref.1, ...), custom_call_target="tpu_custom_call" | custom-call | tf_op jit(solution)/shard_map/layer/pallas_call | solution.py:422
  180.0 3.2 %copy.17 = bf16[1,512,2048]{2,1,0:T(8,128)(2,1)} copy(bf16[1,512,2048]{2,1,0:T(8,128)(2,1)} %bitcast.8) | data formatting | bytes 4194304
where the time goes:
time: 183 us
  Pallas kernels  179 us (98%)
  local copies, waits for them, and re-layouts  3.16 us (2%)
    pallas_call x1, Pallas kernels, fused_body(): pl.pallas_call(functools.partial(layer_kernel, ('rep', 'fs', 'tp')), out_...  179 us

commit v1 on v0

v1 whole, which is shorter than its diff:
```python
import functools
import jax
import jax.numpy as jnp
from jax import lax
from jax.experimental import pallas as pl
from jax.experimental.pallas import tpu as pltpu
from jax.sharding import PartitionSpec as P

EPSILON = 1e-06
RATE_GAIN = 8.0
LANES = 128
SEGMENTS = 8
PAD = 8


def normalize(stream, gain):
    return stream * lax.rsqrt(jnp.mean(stream * stream, axis=-1, keepdims=True) + EPSILON) * gain


def one_minus_exp(y):
    series = 1.0 + y * (1.0 / 6.0)
    for k in (5.0, 4.0, 3.0, 2.0):
        series = 1.0 + y * (1.0 / k) * series
    return jnp.where(y > -0.25, -y * series, 1.0 - jnp.exp(y))


def sigmoid(x):
    return 0.5 * jnp.tanh(0.5 * x) + 0.5


def gate_part(padded, taps_ref, rate_ref, recall_ref, admit_ref, decay, drive, length, serve=None):
    directions, groups, block, _ = recall_ref.shape
    taps = taps_ref.shape[0]
    rows = length // SEGMENTS

    def tile_step(tile, _):
        base = pl.multiple_of(tile * rows, rows)
        conv = jnp.zeros((rows, padded.shape[1]), jnp.float32)
        window = padded[pl.ds(base, rows + 2 * PAD), :]
        for k in range(taps):
            first = PAD - taps // 2 + k
            conv = conv + taps_ref[k : k + 1, :] * window[first : first + rows, :]
        narrow = conv.astype(jnp.bfloat16)
        for g in range(groups):
            values = conv[:, g * block : (g + 1) * block]
            left = narrow[:, g * block : (g + 1) * block]
            for d in range(directions):
                recall = sigmoid(jnp.dot(left, recall_ref[d, g].astype(jnp.bfloat16), preferred_element_type=jnp.float32))
                admit = sigmoid(jnp.dot(left, admit_ref[d, g].astype(jnp.bfloat16), preferred_element_type=jnp.float32))
                log_decay = recall * (-RATE_GAIN * rate_ref[d : d + 1, g * block : (g + 1) * block])
                a = jnp.exp(log_decay)
                b = jnp.sqrt(one_minus_exp(2.0 * log_decay)) * admit * values
                for c in range(block // LANES):
                    where = g * (block // LANES) + c
                    decay[d, where, pl.ds(base, rows), :] = a[:, c * LANES : (c + 1) * LANES]
                    drive[d, where, pl.ds(base, rows), :] = b[:, c * LANES : (c + 1) * LANES]
        return 0

    if serve is None:
        lax.fori_loop(0, SEGMENTS, tile_step, 0)
        return
    for first in range(0, SEGMENTS, 2):
        lax.fori_loop(first, first + 2, tile_step, 0)
        serve()


def scan_part(decay, drive, prefix, mixed_ref, length, serve=None):
    directions, chunks = decay.shape[:2]
    steps = length // SEGMENTS
    lanes = [(d, c) for d in range(directions) for c in range(chunks)]

    def scan_step(s, carried):
        out = []
        for (d, c), (state, product) in zip(lanes, carried):
            at = s if d == 0 else steps - 1 - s
            a = decay[d, c, pl.ds(at, SEGMENTS, stride=steps), :]
            b = drive[d, c, pl.ds(at, SEGMENTS, stride=steps), :]
            state = a * state + b
            product = a * product
            drive[d, c, pl.ds(at, SEGMENTS, stride=steps), :] = state
            prefix[d, c, pl.ds(at, SEGMENTS, stride=steps), :] = product
            out.append((state, product))
        return tuple(out)

    start = tuple((jnp.zeros((SEGMENTS, LANES), jnp.float32), jnp.ones((SEGMENTS, LANES), jnp.float32)) for _ in lanes)
    if serve is None:
        ends = lax.fori_loop(0, steps, scan_step, start, unroll=4)
    else:
        ends = start
        for first in range(0, steps, steps // 4):
            ends = lax.fori_loop(first, first + steps // 4, scan_step, ends, unroll=4)
            serve()
    ends = dict(zip(lanes, ends))

    for c in range(chunks):
        carries = []
        for d in range(directions):
            state, product = ends[(d, c)]
            order = range(SEGMENTS) if d == 0 else range(SEGMENTS - 1, -1, -1)
            carry = jnp.zeros((1, LANES), jnp.float32)
            entering = {}
            for k in order:
                entering[k] = carry
                carry = product[k : k + 1, :] * carry + state[k : k + 1, :]
            carries.append(entering)
        for k in range(SEGMENTS):
            span = pl.ds(k * steps, steps)
            total = drive[0, c, span, :] + prefix[0, c, span, :] * carries[0][k]
            total = total + (drive[1, c, span, :] + prefix[1, c, span, :] * carries[1][k])
            mixed_ref[span, c * LANES : (c + 1) * LANES] = total.astype(jnp.bfloat16)
        if serve is not None:
            serve()


def recurrence_kernel(before_ref, taps_ref, rate_ref, recall_ref, admit_ref, mixed_ref, padded, decay, drive, prefix):
    length, width = before_ref.shape
    edge = jnp.zeros((PAD, width), jnp.float32)
    padded[pl.ds(0, PAD), :] = edge
    padded[pl.ds(PAD + length, PAD), :] = edge
    padded[pl.ds(PAD, length), :] = before_ref[...].astype(jnp.float32)
    gate_part(padded, taps_ref, rate_ref, recall_ref, admit_ref, decay, drive, length)
    scan_part(decay, drive, prefix, mixed_ref, length)


def recurrence(before, taps, rates, recall_maps, admit_maps):
    length, width = before.shape
    directions = rates.shape[0]
    chunks = width // LANES
    plane = pltpu.VMEM((directions, chunks, length, LANES), jnp.float32)
    return pl.pallas_call(
        recurrence_kernel,
        out_shape=jax.ShapeDtypeStruct((length, width), jnp.bfloat16),
        in_specs=[pl.BlockSpec(memory_space=pltpu.VMEM)] * 5,
        out_specs=pl.BlockSpec(memory_space=pltpu.VMEM),
        scratch_shapes=[pltpu.VMEM((length + 2 * PAD, width), jnp.float32), plane, plane, plane],
        compiler_params=pltpu.CompilerParams(vmem_limit_bytes=24 * 2**20),
        cost_estimate=pl.CostEstimate(flops=16 * length * width * 256, bytes_accessed=8 * 2**20, transcendentals=8 * length * width),
        name="recurrence",
    )(before, taps, rates, recall_maps, admit_maps)


def contract_last(left, right):
    return lax.dot_general(
        left, right, (((1,), (1,)), ((), ())), preferred_element_type=jnp.float32
    )


def gather(shard):
    copies = lax.axis_size("rep")
    if shard.shape[0] % (16 * copies):
        return lax.all_gather(shard.astype(jnp.bfloat16), "fs", axis=0, tiled=True)
    rows = shard.shape[0] // copies
    part = lax.dynamic_slice_in_dim(shard, lax.axis_index("rep") * rows, rows, 0)
    return lax.all_gather(part.astype(jnp.bfloat16), ("fs", "rep"), axis=0, tiled=True)


def body(
    tokens,
    first_gain,
    in_matrix,
    in_scale,
    conv_taps,
    decay_rate,
    recall_maps,
    admit_maps,
    out_matrix,
    out_scale,
    second_gain,
    up_matrix,
    up_scale,
    down_matrix,
    down_scale,
):
    stream = tokens.reshape(tokens.shape[1], tokens.shape[2]).astype(jnp.float32)
    factors = lax.all_gather(
        jnp.stack([out_scale, down_scale]).astype(jnp.bfloat16), "fs", axis=1, tiled=True
    )
    in_cols = gather(in_matrix)
    normed = normalize(stream, first_gain).astype(jnp.bfloat16)
    before = (
        jnp.dot(normed, in_cols, preferred_element_type=jnp.float32) * in_scale.astype(jnp.bfloat16)
    ).astype(jnp.bfloat16)
    mixed = recurrence(before, conv_taps, decay_rate, recall_maps, admit_maps)
    partial_value = contract_last(mixed, gather(out_matrix))
    middle = stream + factors[0] * lax.psum(partial_value.astype(jnp.bfloat16), "tp").astype(
        jnp.float32
    )
    second_normed = normalize(middle, second_gain).astype(jnp.bfloat16)
    raised = jnp.dot(second_normed, gather(up_matrix), preferred_element_type=jnp.float32)
    active = jnp.square(jax.nn.relu(raised * up_scale.astype(jnp.bfloat16))).astype(jnp.bfloat16)
    lowered = contract_last(active, gather(down_matrix))
    result = (
        middle + factors[1] * lax.psum(lowered.astype(jnp.bfloat16), "tp").astype(jnp.float32)
    ).astype(jnp.bfloat16)
    return result.reshape(tokens.shape)

MESH = pl.DeviceIdType.MESH
UNITS = 12
AHEAD = 2
EDGE_SERVES = ((), (), (), (), (), (0, 1, 12, 13, 24, 2, 14, 25, 3,), (15,), (), (), (26,), (), (), (4,), (), (16,), (), (27,), (), (), (), (5, 17,), (), (), (), (), (), (28,), (), (), (6,), (), (), (18,), (29,), (7,), (19,), (30,), (8,), (20,), (31,), (), (9,), (), (21,), (), (), (32,), (), (), (10,), (), (22, 33, 11, 23,), (), (), (34,), (), (), (35,), (), (), (), (), (), (), (), (), (), (), ())
INNER_SERVES = ((), (), (), (), (), (0, 12, 1, 13, 2, 24, 3, 14, 4, 25, 5, 15, 6, 26, 7, 16, 8, 27, 9, 17, 10, 28,), (11, 18,), (), (), (29,), (), (), (19,), (), (30,), (), (20,), (), (), (), (31, 21, 32,), (), (22,), (), (), (), (33,), (), (), (), (), (23,), (34,), (35,), (), (), (), (), (), (), (), (), (), (), (), (), (), (), (), (), (), (), (), (), (), (), (), (), (), (), (), (), (), (), (), (), (), (), ())


def layer_kernel(
    names, tokens_hbm, first_ref, in_hbm, in_scale_ref, taps_ref, rate_ref, recall_hbm, admit_hbm,
    out_hbm, out_scale_ref, second_ref, up_hbm, up_scale_ref, down_hbm, down_scale_ref,
    result_ref,
    tokens, in_own, out_own, up_own, down_own, recall_ref, admit_ref,
    in_all, out_all, up_all, down_all, scales_all, normed, second_normed, padded, decay, drive, prefix, mixed, active,
    parts, near_parts, pairs, far_pairs, middle, load, send, recv,
):
    replica, place, rank = (lax.axis_index(name) for name in names)
    rep_name, fs_name, tp_name = names
    fs = 4
    length, model = tokens.shape
    block = model // fs
    half, quarter = block // 2, block // 4
    mate = place + 1 - 2 * lax.rem(place, 2)
    inner = lax.rem(lax.div(place + 1, 2), 2)
    other = fs - 1 - place
    other_mate = fs - 1 - mate
    slots = (mate, inner * other + (1 - inner) * other_mate, inner * other_mate + (1 - inner) * other)
    core = lax.rem(rank, 2)
    near = rank + 1 - 2 * core
    far = lax.rem(rank + 2, 4)
    sends, recvs = [0], [0]

    def fresh(counter):
        counter[0] += 1
        return counter[0] - 1

    def copy(src, dst, axis, peer, into=None):
        index = fresh(recvs) if into is None else into
        return pltpu.make_async_remote_copy(
            src_ref=src, dst_ref=dst, send_sem=send.at[fresh(sends)], recv_sem=recv.at[index],
            device_id={axis: peer}, device_id_type=MESH,
        )

    started, inner_started = [], []

    def start(*copies):
        for one in copies:
            one.start()
            started.append(one)

    loads = [
        pltpu.make_async_copy(src, dst, load.at[i])
        for i, (src, dst) in enumerate((
            (in_hbm, in_own), (out_hbm, out_own), (tokens_hbm, tokens), (up_hbm, up_own), (down_hbm, down_own),
            (recall_hbm, recall_ref), (admit_hbm, admit_ref),
        ))
    ]
    for one in loads:
        one.start()
    load_in, load_out, load_tokens, load_up, load_down, load_recall, load_admit = loads

    barrier = pltpu.get_barrier_semaphore()
    greeted = [(rep_name, 1 - replica)]
    greeted += [(fs_name, lax.rem(place + k, fs)) for k in range(1, fs)]
    greeted += [(tp_name, near), (tp_name, far)]
    for axis, peer in greeted:
        pl.semaphore_signal(barrier, inc=1, device_id={axis: peer}, device_id_type=MESH)

    own_rows = pl.ds(pl.multiple_of(place * block, block), block)
    load_in.wait()
    in_all[own_rows, :] = in_own[...].astype(jnp.bfloat16)
    load_out.wait()
    out_all[own_rows, :] = out_own[...].astype(jnp.bfloat16)
    scales_all[place, 0:1, :] = out_scale_ref[...]
    scales_all[place, 1:2, :] = down_scale_ref[...]

    wide = up_all.shape[1] // 2

    def view(owner, unit):
        def rows(step):
            return pl.ds(pl.multiple_of(owner * block + replica * half + step * quarter, quarter), quarter)

        if unit < 4:
            return (in_all, out_all)[unit // 2].at[rows(unit % 2), :]
        if unit < 8:
            return up_all.at[rows(unit % 2), (unit - 4) // 2 * wide : ((unit - 4) // 2 + 1) * wide]
        return down_all.at[rows((unit - 8) // 2), unit % 2 * wide : (unit % 2 + 1) * wide]

    to_mate, to_other, pass_mate, pass_other, pass_last, swaps = [], [], [], [], [], []
    for unit in range(UNITS):
        into = [fresh(recvs) for _ in range(3)]
        own, first, second, third = (view(owner, unit) for owner in (place,) + slots)
        to_mate.append(copy(own, own, fs_name, mate, into[0]))
        to_other.append(copy(own, own, fs_name, other, into[1]))
        pass_mate.append(copy(first, first, fs_name, other, into[2]))
        pass_other.append(copy(second, second, fs_name, mate, into[1]))
        pass_last.append(copy(third, third, fs_name, mate, into[2]))
        swaps.append([copy(part, part, rep_name, 1 - replica) for part in (first, second, third)])
    arrivals = (to_mate, to_other, pass_last)
    sent = {"mate": 0, "other": 0}

    def start_inner(one):
        one.start()
        inner_started.append(one)

    def serve_edge(codes):
        for code in codes:
            slot, unit = code // UNITS, code % UNITS
            arrivals[slot][unit].wait_recv()
            swaps[unit][slot].start()

    def serve_inner(codes):
        for code in codes:
            slot, unit = code // UNITS, code % UNITS
            arrivals[slot][unit].wait_recv()
            swaps[unit][slot].start()
            if slot == 0:
                start_inner(pass_mate[unit])
                if sent["other"] < UNITS:
                    start_inner(to_other[sent["other"]])
                    sent["other"] += 1
            elif slot == 1:
                start_inner(pass_other[unit])
            else:
                start_inner(pass_last[unit])
                if sent["mate"] < UNITS:
                    to_mate[sent["mate"]].start()
                    sent["mate"] += 1

    point = [0]

    def serve():
        edge_codes, inner_codes = EDGE_SERVES[point[0]], INNER_SERVES[point[0]]
        point[0] += 1
        if edge_codes:
            pl.when(inner == 0)(lambda: serve_edge(edge_codes))
        if inner_codes:
            pl.when(inner == 1)(lambda: serve_inner(inner_codes))

    def need_weights(*units):
        serve()
        for slot in range(3):
            for unit in units:
                swaps[unit][slot].wait_recv()

    pl.semaphore_wait(barrier, len(greeted))

    @pl.when(inner == 0)
    def _():
        for unit in range(4):
            to_mate[unit].start()

    @pl.when(inner == 1)
    def _():
        for unit in range(AHEAD):
            to_mate[unit].start()
            start_inner(to_other[unit])
        sent["mate"] = sent["other"] = AHEAD

    scale_copies = [
        copy(scales_all.at[place], scales_all.at[place], fs_name, lax.rem(place + k, fs)) for k in range(1, fs)
    ]
    start(*scale_copies)
    load_up.wait()
    up_all[own_rows, :] = up_own[...].astype(jnp.bfloat16)
    load_down.wait()
    down_all[own_rows, :] = down_own[...].astype(jnp.bfloat16)

    @pl.when(inner == 0)
    def _():
        for unit in range(4, UNITS):
            to_mate[unit].start()

    load_tokens.wait()
    serve()
    tile = 64
    for i in range(4):

        def norm_step(k, _, i=i):
            at = pl.ds(pl.multiple_of((2 * i + k) * tile, tile), tile)
            normed[at, :] = normalize(tokens[at, :].astype(jnp.float32), first_ref[...]).astype(jnp.bfloat16)
            return 0

        lax.fori_loop(0, length // tile // 4, norm_step, 0)
        serve()

    edge = jnp.zeros((PAD, padded.shape[1]), jnp.float32)
    padded[pl.ds(0, PAD), :] = edge
    padded[pl.ds(PAD + length, PAD), :] = edge
    load_recall.wait()
    load_admit.wait()
    need_weights(0, 1)
    step = 256
    for i in range(in_all.shape[1] // step):
        at = slice(i * step, (i + 1) * step)
        product = jnp.dot(normed[...], in_all[:, at], preferred_element_type=jnp.float32)
        product = product * in_scale_ref[:, at].astype(jnp.bfloat16).astype(jnp.float32)
        padded[pl.ds(PAD, length), at] = product.astype(jnp.bfloat16).astype(jnp.float32)
        serve()
    gate_part(padded, taps_ref, rate_ref, recall_ref, admit_ref, decay, drive, length, serve)
    scan_part(decay, drive, prefix, mixed, length, serve)

    need_weights(2, 3)
    for one in scale_copies:
        one.wait_recv()
    chunks = model // step
    kept = pl.ds(pl.multiple_of(core * (length // 2), length // 2), length // 2)
    given = pl.ds(pl.multiple_of((1 - core) * (length // 2), length // 2), length // 2)

    class Combine:
        def __init__(self, stage):
            self.stage = stage
            self.to_near = [
                copy(parts.at[stage, k, given, :], near_parts.at[stage, k], tp_name, near) for k in range(chunks)
            ]
            self.to_far = [copy(pairs.at[stage, k], far_pairs.at[stage, k], tp_name, far) for k in range(chunks)]

        def put(self, k, partial):
            parts[self.stage, k] = partial.astype(jnp.bfloat16)
            start(self.to_near[k])

        def pair(self, k):
            self.to_near[k].wait_recv()
            total = parts[self.stage, k, kept, :].astype(jnp.float32) + near_parts[self.stage, k].astype(jnp.float32)
            pairs[self.stage, k] = total.astype(jnp.bfloat16)
            start(self.to_far[k])

        def total(self, k):
            self.to_far[k].wait_recv()
            return pairs[self.stage, k].astype(jnp.float32) + far_pairs[self.stage, k].astype(jnp.float32)

    def factor(owner, which, at):
        return scales_all[owner, which : which + 1, at].astype(jnp.bfloat16).astype(jnp.float32)

    one_stage = Combine(0)
    for k in range(chunks + 2):
        if k < chunks:
            one_stage.put(k, contract_last(mixed[...], out_all[k * step : (k + 1) * step, :]))
        serve()
        if k >= 2:
            one_stage.pair(k - 2)
    squares = jnp.zeros((length // 2, 1), jnp.float32)
    for k in range(chunks):
        serve()
        at = slice(k * step, (k + 1) * step)
        inside = slice(k * step % block, k * step % block + step)
        value = tokens[kept, at].astype(jnp.float32) + factor(k * step // block, 0, inside) * one_stage.total(k)
        middle[:, at] = value
        squares = squares + jnp.sum(value * value, axis=1, keepdims=True)
    inverse = lax.rsqrt(squares * (1.0 / model) + EPSILON)
    spreads = []
    for i in range(2):
        rows = slice(i * (length // 4), (i + 1) * (length // 4))
        at = pl.ds(pl.multiple_of(core * (length // 2) + i * (length // 4), length // 4), length // 4)
        second_normed[at, :] = (middle[rows, :] * inverse[rows, :] * second_ref[...]).astype(jnp.bfloat16)
        spreads.append(copy(second_normed.at[at, :], second_normed.at[at, :], tp_name, near))
        start(spreads[i])
    serve()
    for one in spreads:
        one.wait_recv()

    for part in range(2):
        need_weights(4 + 2 * part, 5 + 2 * part)
        for i in range(part * (wide // step), (part + 1) * (wide // step)):
            at = slice(i * step, (i + 1) * step)
            raised = jnp.dot(second_normed[...], up_all[:, at], preferred_element_type=jnp.float32)
            raised = raised * up_scale_ref[:, at].astype(jnp.bfloat16).astype(jnp.float32)
            active[:, at] = jnp.square(jnp.maximum(raised, 0.0)).astype(jnp.bfloat16)
            serve()

    two_stage = Combine(1)
    order = [(place, 0, None), (place, 1, None)] + [(slots[j], q, j) for q in range(2) for j in range(3)]
    finals = []

    def finish(k):
        owner, q, _ = order[k]
        total = two_stage.total(k)
        for h in range(2):
            inside = slice(h * half + q * quarter, h * half + (q + 1) * quarter)
            at = pl.ds(pl.multiple_of(owner * block + h * half + q * quarter, quarter), quarter)
            value = middle[:, at] + factor(owner, 1, inside) * total[:, h * quarter : (h + 1) * quarter]
            result_ref[kept, at] = value.astype(jnp.bfloat16)
            finals.append(copy(result_ref.at[kept, at], result_ref.at[kept, at], tp_name, near))
            start(finals[-1])

    for k in range(chunks + 4):
        if k < chunks:
            owner, q, j = order[k]
            if j is not None:
                serve()
                for unit in (8 + 2 * q, 9 + 2 * q):
                    swaps[unit][j].wait_recv()
            rows = [
                down_all[pl.ds(pl.multiple_of(owner * block + h * half + q * quarter, quarter), quarter), :] for h in range(2)
            ]
            two_stage.put(k, contract_last(active[...], jnp.concatenate(rows, axis=0)))
        if 1 <= k <= chunks:
            serve()
            two_stage.pair(k - 1)
        if k >= 4:
            serve()
            finish(k - 4)
    serve()
    for one in finals:
        one.wait_recv()
    for one in started:
        one.wait_send()
    for unit in range(UNITS):
        to_mate[unit].wait_send()
        for one in swaps[unit]:
            one.wait_send()

    @pl.when(inner == 1)
    def _():
        for one in inner_started:
            one.wait_send()


def fused_body(
    tokens, first_gain, in_matrix, in_scale, conv_taps, decay_rate, recall_maps, admit_maps,
    out_matrix, out_scale, second_gain, up_matrix, up_scale, down_matrix, down_scale,
):
    length, model = tokens.shape[1:]
    width, hidden = in_matrix.shape[1], up_matrix.shape[1]
    fs = lax.axis_size("fs")
    block, step = model // fs, 256
    directions = decay_rate.shape[0]
    plane = pltpu.VMEM((directions, width // LANES, length, LANES), jnp.float32)
    gate = pltpu.VMEM(recall_maps.shape, jnp.float32)
    pieces = pltpu.VMEM((2, model // step, length // 2, step), jnp.bfloat16)
    vmem, hbm = pl.BlockSpec(memory_space=pltpu.VMEM), pl.BlockSpec(memory_space=pl.ANY)
    arrived = UNITS * 6 + 3 + 2 * 2 * (model // step) + 2 + 2 * (model // step)
    result = pl.pallas_call(
        functools.partial(layer_kernel, ("rep", "fs", "tp")),
        out_shape=jax.ShapeDtypeStruct((length, model), jnp.bfloat16),
        in_specs=[hbm, vmem, hbm, vmem, vmem, vmem, hbm, hbm, hbm, vmem, vmem, hbm, vmem, hbm, vmem],
        out_specs=vmem,
        scratch_shapes=[
            pltpu.VMEM((length, model), jnp.bfloat16),
            pltpu.VMEM((block, width), jnp.float32),
            pltpu.VMEM((block, width), jnp.float32),
            pltpu.VMEM((block, hidden), jnp.float32),
            pltpu.VMEM((block, hidden), jnp.float32),
            gate, gate,
            pltpu.VMEM((model, width), jnp.bfloat16),
            pltpu.VMEM((model, width), jnp.bfloat16),
            pltpu.VMEM((model, hidden), jnp.bfloat16),
            pltpu.VMEM((model, hidden), jnp.bfloat16),
            pltpu.VMEM((fs, 2, block), jnp.float32),
            pltpu.VMEM((length, model), jnp.bfloat16),
            pltpu.VMEM((length, model), jnp.bfloat16),
            pltpu.VMEM((length + 2 * PAD, width), jnp.float32),
            plane, plane, plane,
            pltpu.VMEM((length, width), jnp.bfloat16),
            pltpu.VMEM((length, hidden), jnp.bfloat16),
            pltpu.VMEM((2, model // step, length, step), jnp.bfloat16),
            pieces, pieces, pieces,
            pltpu.VMEM((length // 2, model), jnp.float32),
            pltpu.SemaphoreType.DMA((7,)),
            pltpu.SemaphoreType.DMA((arrived + 2 * UNITS,)),
            pltpu.SemaphoreType.DMA((arrived,)),
        ],
        compiler_params=pltpu.CompilerParams(
            collective_id=0, has_side_effects=True, vmem_limit_bytes=61 * 2**20
        ),
        name="layer",
    )(
        tokens.reshape(length, model), first_gain[None], in_matrix, in_scale[None], conv_taps, decay_rate,
        recall_maps, admit_maps, out_matrix, out_scale[None], second_gain[None], up_matrix, up_scale[None], down_matrix,
        down_scale[None],
    )
    return result.reshape(tokens.shape)


def solution(mesh):
    placed = (
        P(("rep", "fs"), None, None),
        P(),
        P("fs", "tp"),
        P("tp"),
        P(None, "tp"),
        P(None, "tp"),
        P(None, "tp", None, None),
        P(None, "tp", None, None),
        P("fs", "tp"),
        P("fs"),
        P(),
        P("fs", "tp"),
        P("tp"),
        P("fs", "tp"),
        P("fs"),
    )
    small = (mesh.shape["rep"], mesh.shape["fs"], mesh.shape["tp"]) == (2, 4, 4)
    return jax.shard_map(
        fused_body if small else body, mesh=mesh, in_specs=placed, out_specs=P(("rep", "fs"), None, None), check_vma=False
    )
```

time: 183 us -> 134 us (0.73)
  Pallas kernels: 179 us -> 131 us
    pallas_call x1, Pallas kernels: 179 us -> 131 us  [fused_body(): pl.pallas_call(functools.partial(layer_kernel, ('rep', 'fs', 'tp')), out_...]
where the time goes in v1:
time: 134 us
  Pallas kernels  131 us (98%)
  local copies, waits for them, and re-layouts  3.16 us (2%)
    pallas_call x1, Pallas kernels, fused_body(): pl.pallas_call(functools.partial(layer_kernel, ('rep', 'fs', 'tp')), out_...  131 us
    unnamed x1, local copies, waits for them, and re-layouts  3.16 us

profile of v1, /device:TPU:0, one launch (start us, length us, event | category | flops | bytes accessed | tf_op | source)
XLA Modules:
  0.0 134.3 jit_solution(364824383196156802)
XLA Ops:
  0.0 131.1 %layer.1 = bf16[512,2048]{1,0:T(8,128)(2,1)} custom-call(bf16[512,2048]{1,0:T(8,128)(2,1)} %bitcast.9, f32[1,2048]{1,0:T(1,128)} %bitcast.10, f32[512,512]{1,0:T(8,128)} %in_hbm.1, f32[1,512]{1,0:T(1,128)} %bitcast.13, f32[4,512]{1,0:T(4,128)} %taps_ref.1, f32[2,512]{1,0:T(2,128)} %rate_ref.1, f32[2,2,256,256]{3,2,1,0:T(8,128)} %recall_hbm.1, ...), custom_call_target="tpu_custom_call" | custom-call | tf_op jit(solution)/shard_map/layer/pallas_call | solution.py:528
  131.1 3.2 %copy.17 = bf16[1,512,2048]{2,1,0:T(8,128)(2,1)} copy(bf16[1,512,2048]{2,1,0:T(8,128)(2,1)} %bitcast.8) | data formatting | bytes 4194304

commit v2 on v1

v2 whole, which is shorter than its diff:
```python
import functools
import jax
import jax.numpy as jnp
from jax import lax
from jax.experimental import pallas as pl
from jax.experimental.pallas import tpu as pltpu
from jax.sharding import PartitionSpec as P

EPSILON = 1e-06
RATE_GAIN = 8.0
LANES = 128
SEGMENTS = 8
PAD = 8
GAP = 8


def normalize(stream, gain):
    return stream * lax.rsqrt(jnp.mean(stream * stream, axis=-1, keepdims=True) + EPSILON) * gain


def one_minus_exp(y):
    series = 1.0 + y * (1.0 / 6.0)
    for k in (5.0, 4.0, 3.0, 2.0):
        series = 1.0 + y * (1.0 / k) * series
    return jnp.where(y > -0.25, -y * series, 1.0 - jnp.exp(y))


def sigmoid(x):
    return 0.5 * jnp.tanh(0.5 * x) + 0.5


def gate_part(padded, taps_ref, rate_ref, recall_ref, admit_ref, decay, drive, length, serve=None):
    directions, groups, block, _ = recall_ref.shape
    taps = taps_ref.shape[0]
    rows = length // SEGMENTS
    pitch = decay.shape[2] // SEGMENTS

    def tile_step(tile, _):
        base = pl.multiple_of(tile * rows, rows)
        into = pl.multiple_of(tile * pitch, 8)
        conv = jnp.zeros((rows, padded.shape[1]), jnp.float32)
        window = padded[pl.ds(base, rows + 2 * PAD), :]
        for k in range(taps):
            first = PAD - taps // 2 + k
            conv = conv + taps_ref[k : k + 1, :] * window[first : first + rows, :]
        narrow = conv.astype(jnp.bfloat16)
        for g in range(groups):
            values = conv[:, g * block : (g + 1) * block]
            left = narrow[:, g * block : (g + 1) * block]
            for d in range(directions):
                recall = sigmoid(jnp.dot(left, recall_ref[d, g].astype(jnp.bfloat16), preferred_element_type=jnp.float32))
                admit = sigmoid(jnp.dot(left, admit_ref[d, g].astype(jnp.bfloat16), preferred_element_type=jnp.float32))
                log_decay = recall * (-RATE_GAIN * rate_ref[d : d + 1, g * block : (g + 1) * block])
                a = jnp.exp(log_decay)
                b = jnp.sqrt(one_minus_exp(2.0 * log_decay)) * admit * values
                for c in range(block // LANES):
                    where = g * (block // LANES) + c
                    decay[d, where, pl.ds(into, rows), :] = a[:, c * LANES : (c + 1) * LANES]
                    drive[d, where, pl.ds(into, rows), :] = b[:, c * LANES : (c + 1) * LANES]
        return 0

    if serve is None:
        lax.fori_loop(0, SEGMENTS, tile_step, 0)
        return
    for first in range(0, SEGMENTS, 2):
        lax.fori_loop(first, first + 2, tile_step, 0)
        serve()


def scan_part(decay, drive, prefix, mixed_ref, length, serve=None):
    directions, chunks = decay.shape[:2]
    steps = length // SEGMENTS
    pitch = decay.shape[2] // SEGMENTS
    lanes = [(d, c) for d in range(directions) for c in range(chunks)]

    def scan_step(s, carried):
        out = []
        for (d, c), (state, product) in zip(lanes, carried):
            at = s if d == 0 else steps - 1 - s
            a = decay[d, c, pl.ds(at, SEGMENTS, stride=pitch), :]
            b = drive[d, c, pl.ds(at, SEGMENTS, stride=pitch), :]
            state = a * state + b
            product = a * product
            drive[d, c, pl.ds(at, SEGMENTS, stride=pitch), :] = state
            prefix[d, c, pl.ds(at, SEGMENTS, stride=pitch), :] = product
            out.append((state, product))
        return tuple(out)

    start = tuple((jnp.zeros((SEGMENTS, LANES), jnp.float32), jnp.ones((SEGMENTS, LANES), jnp.float32)) for _ in lanes)
    if serve is None:
        ends = lax.fori_loop(0, steps, scan_step, start, unroll=4)
    else:
        ends = start
        for first in range(0, steps, steps // 4):
            ends = lax.fori_loop(first, first + steps // 4, scan_step, ends, unroll=4)
            serve()
    ends = dict(zip(lanes, ends))

    for c in range(chunks):
        carries = []
        for d in range(directions):
            state, product = ends[(d, c)]
            order = range(SEGMENTS) if d == 0 else range(SEGMENTS - 1, -1, -1)
            carry = jnp.zeros((1, LANES), jnp.float32)
            entering = {}
            for k in order:
                entering[k] = carry
                carry = product[k : k + 1, :] * carry + state[k : k + 1, :]
            carries.append(entering)
        for k in range(SEGMENTS):
            span = pl.ds(k * pitch, steps)
            total = drive[0, c, span, :] + prefix[0, c, span, :] * carries[0][k]
            total = total + (drive[1, c, span, :] + prefix[1, c, span, :] * carries[1][k])
            mixed_ref[pl.ds(k * steps, steps), c * LANES : (c + 1) * LANES] = total.astype(jnp.bfloat16)
        if serve is not None:
            serve()


def recurrence_kernel(before_ref, taps_ref, rate_ref, recall_ref, admit_ref, mixed_ref, padded, decay, drive, prefix):
    length, width = before_ref.shape
    edge = jnp.zeros((PAD, width), jnp.float32)
    padded[pl.ds(0, PAD), :] = edge
    padded[pl.ds(PAD + length, PAD), :] = edge
    padded[pl.ds(PAD, length), :] = before_ref[...].astype(jnp.float32)
    gate_part(padded, taps_ref, rate_ref, recall_ref, admit_ref, decay, drive, length)
    scan_part(decay, drive, prefix, mixed_ref, length)


def recurrence(before, taps, rates, recall_maps, admit_maps):
    length, width = before.shape
    directions = rates.shape[0]
    chunks = width // LANES
    plane = pltpu.VMEM((directions, chunks, length, LANES), jnp.float32)
    return pl.pallas_call(
        recurrence_kernel,
        out_shape=jax.ShapeDtypeStruct((length, width), jnp.bfloat16),
        in_specs=[pl.BlockSpec(memory_space=pltpu.VMEM)] * 5,
        out_specs=pl.BlockSpec(memory_space=pltpu.VMEM),
        scratch_shapes=[pltpu.VMEM((length + 2 * PAD, width), jnp.float32), plane, plane, plane],
        compiler_params=pltpu.CompilerParams(vmem_limit_bytes=24 * 2**20),
        cost_estimate=pl.CostEstimate(flops=16 * length * width * 256, bytes_accessed=8 * 2**20, transcendentals=8 * length * width),
        name="recurrence",
    )(before, taps, rates, recall_maps, admit_maps)


def contract_last(left, right):
    return lax.dot_general(
        left, right, (((1,), (1,)), ((), ())), preferred_element_type=jnp.float32
    )


def gather(shard):
    copies = lax.axis_size("rep")
    if shard.shape[0] % (16 * copies):
        return lax.all_gather(shard.astype(jnp.bfloat16), "fs", axis=0, tiled=True)
    rows = shard.shape[0] // copies
    part = lax.dynamic_slice_in_dim(shard, lax.axis_index("rep") * rows, rows, 0)
    return lax.all_gather(part.astype(jnp.bfloat16), ("fs", "rep"), axis=0, tiled=True)


def body(
    tokens,
    first_gain,
    in_matrix,
    in_scale,
    conv_taps,
    decay_rate,
    recall_maps,
    admit_maps,
    out_matrix,
    out_scale,
    second_gain,
    up_matrix,
    up_scale,
    down_matrix,
    down_scale,
):
    stream = tokens.reshape(tokens.shape[1], tokens.shape[2]).astype(jnp.float32)
    factors = lax.all_gather(
        jnp.stack([out_scale, down_scale]).astype(jnp.bfloat16), "fs", axis=1, tiled=True
    )
    in_cols = gather(in_matrix)
    normed = normalize(stream, first_gain).astype(jnp.bfloat16)
    before = (
        jnp.dot(normed, in_cols, preferred_element_type=jnp.float32) * in_scale.astype(jnp.bfloat16)
    ).astype(jnp.bfloat16)
    mixed = recurrence(before, conv_taps, decay_rate, recall_maps, admit_maps)
    partial_value = contract_last(mixed, gather(out_matrix))
    middle = stream + factors[0] * lax.psum(partial_value.astype(jnp.bfloat16), "tp").astype(
        jnp.float32
    )
    second_normed = normalize(middle, second_gain).astype(jnp.bfloat16)
    raised = jnp.dot(second_normed, gather(up_matrix), preferred_element_type=jnp.float32)
    active = jnp.square(jax.nn.relu(raised * up_scale.astype(jnp.bfloat16))).astype(jnp.bfloat16)
    lowered = contract_last(active, gather(down_matrix))
    result = (
        middle + factors[1] * lax.psum(lowered.astype(jnp.bfloat16), "tp").astype(jnp.float32)
    ).astype(jnp.bfloat16)
    return result.reshape(tokens.shape)

MESH = pl.DeviceIdType.MESH
UNITS = 12
SPLIT = 2
OWN_TO_MATE = (2, 3, 4, 5, 6, 7, 8, 9)
OWN_TO_MATE_AFTER = {4: (10,), 7: (11,)}
OWN_TO_OTHER = (0, 1)
OWN_TO_OTHER_AFTER = {1: (2, 3), 3: (4, 5, 6), 6: (7,), 7: (8, 9, 10), 10: (11,)}
EDGE_SENDS = ((1, 2), (1, 3), (0, 2), (0, 3), (1, 4), (1, 5), (1, 6), (1, 7), (0, 4), (0, 5), (0, 6), (0, 7), (1, 8), (1, 9), (1, 10), (1, 11), (0, 8), (0, 9), (0, 10), (0, 11))
DOWN_ORDER = ((0, 0), (0, 1), None, (1, 0), (1, 1), (0, 2), (1, 2), (0, 3), (1, 3), (0, 4), (1, 4), (0, 5), (1, 5), (0, 6), (1, 6), (0, 7), (1, 7))
LAG = 8
EDGE_SERVES = (
    (2, 3, 4, 5, 6, 7, 8, 9, 14, 15),
    (),
    (),
    (26,),
    (),
    (27,),
    (),
    (),
    (),
    (16,),
    (),
    (),
    (),
    (17,),
    (),
    (),
    (),
    (),
    (),
    (18,),
    (),
    (),
    (),
    (28,),
    (),
    (),
    (),
    (10,),
    (),
    (29,),
    (),
    (30,),
    (19,),
    (),
    (),
    (),
    (31, 11, 20),
    (),
    (),
    (),
    (),
    (),
    (),
    (),
    (),
    (),
    (),
    (21,),
    (),
    (),
    (),
    (),
    (),
    (22,),
    (),
    (),
    (),
    (),
    (),
    (32,),
    (),
    (),
    (),
    (33, 34, 23),
    (),
    (),
    (),
    (),
    (),
    (),
    (),
    (35,),
    (),
    (),
    (),
    (),
    (),
    (),
    (),
    (),
    (),
    (),
    (),
    (),
    (),
    (),
    (),
    (),
    (),
    (),
    (),
    (),
    (),
)
INNER_SERVES = (
    (),
    (),
    (),
    (),
    (0, 12, 1, 13),
    (24, 25),
    (14,),
    (15,),
    (),
    (),
    (),
    (2,),
    (3,),
    (),
    (),
    (26,),
    (),
    (),
    (27,),
    (),
    (),
    (16, 4),
    (),
    (),
    (17, 5),
    (),
    (),
    (),
    (),
    (),
    (18,),
    (),
    (6,),
    (),
    (),
    (28,),
    (),
    (),
    (7,),
    (),
    (),
    (29,),
    (),
    (30,),
    (),
    (19,),
    (),
    (31,),
    (20, 8),
    (),
    (),
    (),
    (21,),
    (),
    (9,),
    (),
    (),
    (),
    (),
    (),
    (22, 10),
    (),
    (32, 11),
    (33,),
    (),
    (),
    (),
    (),
    (),
    (),
    (),
    (),
    (34,),
    (),
    (),
    (),
    (),
    (),
    (23,),
    (),
    (),
    (),
    (35,),
    (),
    (),
    (),
    (),
    (),
    (),
    (),
    (),
    (),
    (),
    (),
    (),
    (),
    (),
    (),
    (),
    (),
    (),
    (),
    (),
    (),
    (),
    (),
    (),
    (),
    (),
)


def layer_kernel(
    names, tokens_hbm, first_ref, in_hbm, in_scale_ref, taps_ref, rate_ref, recall_hbm, admit_hbm,
    out_hbm, out_scale_ref, second_ref, up_hbm, up_scale_ref, down_hbm, down_scale_ref,
    result_ref,
    tokens, in_own, out_own, up_own, down_own, recall_ref, admit_ref,
    in_all, out_all, up_all, down_all, scales_all, normed, guest, before, second_normed, padded, decay, drive, prefix,
    mixed, active, parts, near_parts, pairs, far_pairs, middle, load, send, recv,
):
    replica, place, rank = (lax.axis_index(name) for name in names)
    rep_name, fs_name, tp_name = names
    fs = 4
    length, model = tokens.shape
    block = model // fs
    half, quarter = block // 2, block // 4
    mate = place + 1 - 2 * lax.rem(place, 2)
    inner = lax.rem(lax.div(place + 1, 2), 2)
    other = fs - 1 - place
    other_mate = fs - 1 - mate
    slots = (mate, inner * other + (1 - inner) * other_mate, inner * other_mate + (1 - inner) * other)
    core = lax.rem(rank, 2)
    near = rank + 1 - 2 * core
    far = lax.rem(rank + 2, 4)
    sends, recvs = [0], [0]

    def fresh(counter):
        counter[0] += 1
        return counter[0] - 1

    def copy(src, dst, axis, peer, into=None):
        index = fresh(recvs) if into is None else into
        return pltpu.make_async_remote_copy(
            src_ref=src, dst_ref=dst, send_sem=send.at[fresh(sends)], recv_sem=recv.at[index],
            device_id={axis: peer}, device_id_type=MESH,
        )

    common_sent, edge_sent, inner_sent = [], [], []

    def start(one, sent=common_sent):
        one.start()
        sent.append(one)

    loads = [
        pltpu.make_async_copy(src, dst, load.at[i])
        for i, (src, dst) in enumerate((
            (in_hbm, in_own), (tokens_hbm, tokens), (out_hbm, out_own), (up_hbm, up_own), (down_hbm, down_own),
            (recall_hbm, recall_ref), (admit_hbm, admit_ref),
        ))
    ]
    for one in loads:
        one.start()
    load_in, load_tokens, load_out, load_up, load_down, load_recall, load_admit = loads

    barrier = pltpu.get_barrier_semaphore()
    greeted = [(rep_name, 1 - replica)]
    greeted += [(fs_name, lax.rem(place + k, fs)) for k in range(1, fs)]
    greeted += [(tp_name, near), (tp_name, far)]
    for axis, peer in greeted:
        pl.semaphore_signal(barrier, inc=1, device_id={axis: peer}, device_id_type=MESH)

    own_rows = pl.ds(pl.multiple_of(place * block, block), block)
    load_in.wait()
    in_all[own_rows, :] = in_own[...].astype(jnp.bfloat16)
    scales_all[place, 0:1, :] = out_scale_ref[...]
    scales_all[place, 1:2, :] = down_scale_ref[...]

    wide = up_all.shape[1] // 2

    def view(owner, unit, side):
        def rows(step):
            return pl.ds(pl.multiple_of(owner * block + side * half + step * quarter, quarter), quarter)

        if unit < 4:
            return (in_all, out_all)[unit // 2].at[rows(unit % 2), :]
        if unit < 8:
            return up_all.at[rows(unit % 2), (unit - 4) // 2 * wide : ((unit - 4) // 2 + 1) * wide]
        return down_all.at[rows((unit - 8) // 2), unit % 2 * wide : (unit % 2 + 1) * wide]

    to_mate, extra, to_other, pass_mate, pass_other, pass_last, swaps = [], [], [], [], [], [], []
    for unit in range(UNITS):
        into = [fresh(recvs) for _ in range(6)]
        own, first, second, third = (view(owner, unit, replica) for owner in (place,) + slots)
        rest = view(place, unit, 1 - replica)
        to_mate.append(copy(own, own, fs_name, mate, into[0]))
        extra.append(copy(rest, rest, fs_name, mate, into[3]))
        to_other.append(copy(own, own, fs_name, other, into[1]))
        pass_mate.append(copy(first, first, fs_name, other, into[2]))
        pass_other.append(copy(second, second, fs_name, mate, into[1]))
        pass_last.append(copy(third, third, fs_name, mate, into[2]))
        swaps.append([copy(part, part, rep_name, 1 - replica, into[3 + j]) for j, part in enumerate((first, second, third))])
    arrivals = (to_mate, to_other, pass_last)

    def serve_edge(codes):
        for code in codes:
            slot, unit = code // UNITS, code % UNITS
            arrivals[slot][unit].wait_recv()
            start(swaps[unit][slot], edge_sent)

    def serve_inner(codes):
        for code in codes:
            slot, unit = code // UNITS, code % UNITS
            arrivals[slot][unit].wait_recv()
            if slot or unit < SPLIT:
                start(swaps[unit][slot], inner_sent)
            if slot == 0:
                start(pass_mate[unit], inner_sent)
                for u in OWN_TO_OTHER_AFTER.get(unit, ()):
                    start(to_other[u], inner_sent)
            elif unit >= SPLIT:
                start((pass_other, pass_last)[slot - 1][unit], inner_sent)
            if slot == 2:
                for u in OWN_TO_MATE_AFTER.get(unit, ()):
                    start(to_mate[u], inner_sent)

    points = {"edge": 0, "inner": 0}

    def edge_next():
        points["edge"] += 1
        return EDGE_SERVES[points["edge"] - 1]

    def inner_next():
        points["inner"] += 1
        return INNER_SERVES[points["inner"] - 1]

    def serve():
        edge_codes, inner_codes = edge_next(), inner_next()
        if edge_codes:
            pl.when(inner == 0)(lambda: serve_edge(edge_codes))
        if inner_codes:
            pl.when(inner == 1)(lambda: serve_inner(inner_codes))

    def landed(units, taken=(0, 1, 2)):
        for unit in units:
            for slot in taken:
                swaps[unit][slot].wait_recv()

    piece = 32
    pieces = length // 4 // piece

    def guest_rows(owner, i):
        return pl.ds(pl.multiple_of(owner * (length // 4) + i * piece, piece), piece)

    tok, tok_far, tok_near, tok_onward = [], [], [], []
    for i in range(pieces):
        mine, theirs = guest_rows(rank, i), guest_rows(far, i)
        tok.append(copy(normed.at[mine, :], guest.at[mine, :], fs_name, mate))
        tok_far.append(copy(guest.at[mine, :], guest.at[mine, :], tp_name, far))
        tok_near.append(copy(guest.at[mine, :], guest.at[mine, :], tp_name, near))
        tok_onward.append(copy(guest.at[theirs, :], guest.at[theirs, :], tp_name, near))
    step = 256
    tiles = [slice(i * step, (i + 1) * step) for i in range(in_all.shape[1] // step)]
    given_before = [copy(before.at[:, at], before.at[:, at], fs_name, mate) for at in tiles]

    pl.semaphore_wait(barrier, len(greeted))

    @pl.when(inner == 0)
    def _():
        for unit in range(SPLIT):
            start(to_mate[unit], edge_sent)

    @pl.when(inner == 1)
    def _():
        for unit in OWN_TO_OTHER:
            start(to_other[unit], inner_sent)

    scale_copies = [
        copy(scales_all.at[place], scales_all.at[place], fs_name, lax.rem(place + k, fs)) for k in range(1, fs)
    ]
    for one in scale_copies:
        start(one)

    def norm_rows(at):
        normed[at, :] = normalize(tokens[at, :].astype(jnp.float32), first_ref[...]).astype(jnp.bfloat16)

    load_tokens.wait()

    @pl.when(inner == 0)
    def _():
        for i in range(pieces):
            norm_rows(guest_rows(rank, i))
            start(tok[i], edge_sent)

    load_out.wait()
    out_all[own_rows, :] = out_own[...].astype(jnp.bfloat16)

    @pl.when(inner == 1)
    def _():
        for unit in OWN_TO_MATE:
            if unit < 4:
                start(to_mate[unit], inner_sent)

    load_up.wait()
    up_all[own_rows, :] = up_own[...].astype(jnp.bfloat16)
    load_down.wait()
    down_all[own_rows, :] = down_own[...].astype(jnp.bfloat16)
    load_recall.wait()
    load_admit.wait()
    edge = jnp.zeros((PAD, padded.shape[1]), jnp.float32)
    padded[pl.ds(0, PAD), :] = edge
    padded[pl.ds(PAD + length, PAD), :] = edge

    @pl.when(inner == 0)
    def _():
        for whole, unit in EDGE_SENDS:
            start((to_mate if whole else extra)[unit], edge_sent)
        serve_edge(edge_next())
        for one, at in zip(given_before, tiles):
            one.wait_recv()
            padded[pl.ds(PAD, length), at] = before[:, at].astype(jnp.float32)

    @pl.when(inner == 1)
    def _():
        for unit in OWN_TO_MATE:
            if unit >= 4:
                start(to_mate[unit], inner_sent)
        tile = 64
        for i in range(4):

            def norm_step(k, _, i=i):
                norm_rows(pl.ds(pl.multiple_of((2 * i + k) * tile, tile), tile))
                return 0

            lax.fori_loop(0, length // tile // 4, norm_step, 0)
            serve_inner(inner_next())
        for i in range(pieces):
            serve_inner(inner_next())
            tok[i].wait_recv()
            start(tok_far[i], inner_sent)
            start(tok_near[i], inner_sent)
        for i in range(pieces):
            serve_inner(inner_next())
            tok_far[i].wait_recv()
            start(tok_onward[i], inner_sent)
        serve_inner(inner_next())
        landed(range(SPLIT))
        for one in tok_near + tok_onward:
            one.wait_recv()

        def project_in(values, at):
            product = jnp.dot(values[...], in_all[:, at], preferred_element_type=jnp.float32)
            return (product * in_scale_ref[:, at].astype(jnp.bfloat16).astype(jnp.float32)).astype(jnp.bfloat16)

        for one, at in zip(given_before, tiles):
            before[:, at] = project_in(guest, at)
            start(one, inner_sent)
            serve_inner(inner_next())
        for at in tiles:
            padded[pl.ds(PAD, length), at] = project_in(normed, at).astype(jnp.float32)
            serve_inner(inner_next())

    gate_part(padded, taps_ref, rate_ref, recall_ref, admit_ref, decay, drive, length, serve)
    scan_part(decay, drive, prefix, mixed, length, serve)

    serve()
    landed((2, 3))
    for one in scale_copies:
        one.wait_recv()
    chunks = model // step
    rows = length // 2
    batch = rows // 2
    kept = pl.ds(pl.multiple_of(core * rows, rows), rows)
    given = pl.ds(pl.multiple_of((1 - core) * rows, rows), rows)

    def of_batch(h):
        return slice(h * batch, (h + 1) * batch)

    def factor(owner, which, at):
        return scales_all[owner, which : which + 1, at].astype(jnp.bfloat16).astype(jnp.float32)

    to_near = [copy(parts.at[0, k, given, :], near_parts.at[0, k], tp_name, near) for k in range(chunks)]
    to_far = [
        [
            [copy(pairs.at[stage, k, of_batch(h), :], far_pairs.at[stage, k, of_batch(h), :], tp_name, far) for k in range(chunks)]
            for h in range(2)
        ]
        for stage in range(2)
    ]

    def far_total(stage, h, k):
        to_far[stage][h][k].wait_recv()
        return pairs[stage, k, of_batch(h), :].astype(jnp.float32) + far_pairs[stage, k, of_batch(h), :].astype(jnp.float32)

    for k in range(chunks + 2):
        if k < chunks:
            product = contract_last(mixed[...], out_all[k * step : (k + 1) * step, :])
            parts[0, k] = product.astype(jnp.bfloat16)
            start(to_near[k])
        serve()
        if k >= 2:
            to_near[k - 2].wait_recv()
            total = parts[0, k - 2, kept, :].astype(jnp.float32) + near_parts[0, k - 2].astype(jnp.float32)
            pairs[0, k - 2] = total.astype(jnp.bfloat16)
            start(to_far[0][0][k - 2])
    for k in range(chunks):
        start(to_far[0][1][k])

    spreads = []

    def middle_rows(h):
        squares = jnp.zeros((batch, 1), jnp.float32)
        at_rows = pl.ds(pl.multiple_of(core * rows + h * batch, batch), batch)
        for k in range(chunks):
            serve()
            at = slice(k * step, (k + 1) * step)
            inside = slice(k * step % block, k * step % block + step)
            value = tokens[at_rows, at].astype(jnp.float32) + factor(k * step // block, 0, inside) * far_total(0, h, k)
            middle[of_batch(h), at] = value
            squares = squares + jnp.sum(value * value, axis=1, keepdims=True)
        inverse = lax.rsqrt(squares * (1.0 / model) + EPSILON)
        at = pl.ds(pl.multiple_of(h * rows + core * batch, batch), batch)
        second_normed[at, :] = (middle[of_batch(h), :] * inverse * second_ref[...]).astype(jnp.bfloat16)
        spreads.append(copy(second_normed.at[at, :], second_normed.at[at, :], tp_name, near))
        start(spreads[h])

    def up_rows(h):
        serve()
        spreads[h].wait_recv()
        at_rows = slice(h * rows, (h + 1) * rows)
        for part in range(2):
            serve()
            if h == 0:
                landed((4 + 2 * part, 5 + 2 * part))
            for i in range(part * (wide // step), (part + 1) * (wide // step)):
                at = slice(i * step, (i + 1) * step)
                raised = jnp.dot(second_normed[at_rows, :], up_all[:, at], preferred_element_type=jnp.float32)
                raised = raised * up_scale_ref[:, at].astype(jnp.bfloat16).astype(jnp.float32)
                active[at_rows, at] = jnp.square(jnp.maximum(raised, 0.0)).astype(jnp.bfloat16)
                serve()

    middle_rows(0)
    up_rows(0)
    middle_rows(1)

    owners = [(place, 0, None), (place, 1, None)] + [(slots[j], q, j) for q in range(2) for j in range(3)]
    turns = [turn for turn in DOWN_ORDER if turn is not None]
    down_near, finals = [], []

    def pair_down(n):
        h, k = turns[n]
        serve()
        down_near[n].wait_recv()
        at = pl.ds(pl.multiple_of(h * rows + core * batch, batch), batch)
        total = parts[1, k, at, :].astype(jnp.float32) + near_parts[1, k, of_batch(h), :].astype(jnp.float32)
        pairs[1, k, of_batch(h), :] = total.astype(jnp.bfloat16)
        start(to_far[1][h][k])

    def finish(n):
        h, k = turns[n]
        owner, q, _ = owners[k]
        serve()
        total = far_total(1, h, k)
        at_rows = pl.ds(pl.multiple_of(core * rows + h * batch, batch), batch)
        for s in range(2):
            inside = slice(s * half + q * quarter, s * half + (q + 1) * quarter)
            at = pl.ds(pl.multiple_of(owner * block + s * half + q * quarter, quarter), quarter)
            value = middle[of_batch(h), at] + factor(owner, 1, inside) * total[:, s * quarter : (s + 1) * quarter]
            result_ref[at_rows, at] = value.astype(jnp.bfloat16)
            finals.append(copy(result_ref.at[at_rows, at], result_ref.at[at_rows, at], tp_name, near))
            start(finals[-1])

    n = 0
    for turn in DOWN_ORDER:
        if turn is None:
            up_rows(1)
            continue
        h, k = turn
        owner, q, j = owners[k]
        if j is not None and h == 0:
            serve()
            landed((8 + 2 * q, 9 + 2 * q), (j,))
        matrix = [
            down_all[pl.ds(pl.multiple_of(owner * block + s * half + q * quarter, quarter), quarter), :] for s in range(2)
        ]
        product = contract_last(active[h * rows : (h + 1) * rows, :], jnp.concatenate(matrix, axis=0))
        parts[1, k, h * rows : (h + 1) * rows, :] = product.astype(jnp.bfloat16)
        away = pl.ds(pl.multiple_of(h * rows + (1 - core) * batch, batch), batch)
        down_near.append(copy(parts.at[1, k, away, :], near_parts.at[1, k, of_batch(h), :], tp_name, near))
        start(down_near[n])
        if n >= 1:
            pair_down(n - 1)
        if n >= LAG:
            finish(n - LAG)
        n += 1
    pair_down(n - 1)
    for m in range(n - LAG, n):
        finish(m)
    serve()
    for one in finals:
        one.wait_recv()
    for one in common_sent:
        one.wait_send()

    @pl.when(inner == 0)
    def _():
        for one in edge_sent:
            one.wait_send()

    @pl.when(inner == 1)
    def _():
        for one in inner_sent:
            one.wait_send()


def fused_body(
    tokens, first_gain, in_matrix, in_scale, conv_taps, decay_rate, recall_maps, admit_maps,
    out_matrix, out_scale, second_gain, up_matrix, up_scale, down_matrix, down_scale,
):
    length, model = tokens.shape[1:]
    width, hidden = in_matrix.shape[1], up_matrix.shape[1]
    fs = lax.axis_size("fs")
    block, step = model // fs, 256
    directions = decay_rate.shape[0]
    plane = pltpu.VMEM((directions, width // LANES, SEGMENTS * (length // SEGMENTS + GAP), LANES), jnp.float32)
    gate = pltpu.VMEM(recall_maps.shape, jnp.float32)
    pieces = pltpu.VMEM((2, model // step, length // 2, step), jnp.bfloat16)
    rows = pltpu.VMEM((length, model), jnp.bfloat16)
    channels = pltpu.VMEM((length, width), jnp.bfloat16)
    vmem, hbm = pl.BlockSpec(memory_space=pltpu.VMEM), pl.BlockSpec(memory_space=pl.ANY)
    count = UNITS * 7 + 3 + 16 + 2 + 9 * (model // step) + 2 + 4 * (model // step)
    result = pl.pallas_call(
        functools.partial(layer_kernel, ("rep", "fs", "tp")),
        out_shape=pltpu.VMEM((length, model), jnp.bfloat16),
        in_specs=[hbm, vmem, hbm, vmem, vmem, vmem, hbm, hbm, hbm, vmem, vmem, hbm, vmem, hbm, vmem],
        out_specs=vmem,
        scratch_shapes=[
            rows,
            pltpu.VMEM((block, width), jnp.float32),
            pltpu.VMEM((block, width), jnp.float32),
            pltpu.VMEM((block, hidden), jnp.float32),
            pltpu.VMEM((block, hidden), jnp.float32),
            gate, gate,
            pltpu.VMEM((model, width), jnp.bfloat16),
            pltpu.VMEM((model, width), jnp.bfloat16),
            pltpu.VMEM((model, hidden), jnp.bfloat16),
            pltpu.VMEM((model, hidden), jnp.bfloat16),
            pltpu.VMEM((fs, 2, block), jnp.float32),
            rows, rows, channels, rows,
            pltpu.VMEM((length + 2 * PAD, width), jnp.float32),
            plane, plane, plane,
            channels,
            pltpu.VMEM((length, hidden), jnp.bfloat16),
            pltpu.VMEM((2, model // step, length, step), jnp.bfloat16),
            pieces, pieces, pieces,
            pltpu.VMEM((length // 2, model), jnp.float32),
            pltpu.SemaphoreType.DMA((7,)),
            pltpu.SemaphoreType.DMA((count + 3 * UNITS,)),
            pltpu.SemaphoreType.DMA((count,)),
        ],
        compiler_params=pltpu.CompilerParams(
            collective_id=0, has_side_effects=True, vmem_limit_bytes=59 * 2**20
        ),
        name="layer",
    )(
        tokens.reshape(length, model), first_gain[None], in_matrix, in_scale[None], conv_taps, decay_rate,
        recall_maps, admit_maps, out_matrix, out_scale[None], second_gain[None], up_matrix, up_scale[None], down_matrix,
        down_scale[None],
    )
    return result.reshape(tokens.shape)


def solution(mesh):
    placed = (
        P(("rep", "fs"), None, None),
        P(),
        P("fs", "tp"),
        P("tp"),
        P(None, "tp"),
        P(None, "tp"),
        P(None, "tp", None, None),
        P(None, "tp", None, None),
        P("fs", "tp"),
        P("fs"),
        P(),
        P("fs", "tp"),
        P("tp"),
        P("fs", "tp"),
        P("fs"),
    )
    small = (mesh.shape["rep"], mesh.shape["fs"], mesh.shape["tp"]) == (2, 4, 4)
    return jax.shard_map(
        fused_body if small else body, mesh=mesh, in_specs=placed, out_specs=P(("rep", "fs"), None, None), check_vma=False
    )
```

time: 134 us -> 123 us (0.918)
  Pallas kernels: 131 us -> 122 us
  local copies, waits for them, and re-layouts: 3.16 us -> 1.32 us
    pallas_call x1, Pallas kernels: 131 us -> 122 us  [fused_body(): pl.pallas_call(functools.partial(layer_kernel, ('rep', 'fs', 'tp')), out_...]
    unnamed x1, local copies, waits for them, and re-layouts: 3.16 us -> 1.32 us
where the time goes in v2:
time: 123 us
  Pallas kernels  122 us (99%)
  local copies, waits for them, and re-layouts  1.32 us (1%)
    pallas_call x1, Pallas kernels, fused_body(): pl.pallas_call(functools.partial(layer_kernel, ('rep', 'fs', 'tp')), out_...  122 us

profile of v2, /device:TPU:0, one launch (start us, length us, event | category | flops | bytes accessed | tf_op | source)
XLA Modules:
  0.0 123.3 jit_solution(13539165940033481901)
XLA Ops:
  0.0 122.0 %layer.1 = bf16[512,2048]{1,0:T(8,128)(2,1)S(1)} custom-call(bf16[512,2048]{1,0:T(8,128)(2,1)} %bitcast.9, f32[1,2048]{1,0:T(1,128)} %bitcast.10, f32[512,512]{1,0:T(8,128)} %in_hbm.1, f32[1,512]{1,0:T(1,128)} %bitcast.13, f32[4,512]{1,0:T(4,128)} %taps_ref.1, f32[2,512]{1,0:T(2,128)} %rate_ref.1, f32[2,2,256,256]{3,2,1,0:T(8,128)} %recall_hbm.1, ...), custom_call_target="tpu_custom_call" | custom-call | tf_op jit(solution)/shard_map/layer/pallas_call | solution.py:837
  122.0 1.3 %copy.17 = bf16[1,512,2048]{2,1,0:T(8,128)(2,1)} copy(bf16[1,512,2048]{2,1,0:T(8,128)(2,1)S(1)} %bitcast.8) | data formatting | bytes 4194304

commit v3 on v2

--- a/solution.py
+++ b/solution.py
@@ -1,4 +1,5 @@
 import functools
+import math
 import jax
 import jax.numpy as jnp
 from jax import lax
@@ -199,90 +200,90 @@
     return result.reshape(tokens.shape)
 
 MESH = pl.DeviceIdType.MESH
-UNITS = 12
+UNITS = 14
 SPLIT = 2
-OWN_TO_MATE = (2, 3, 4, 5, 6, 7, 8, 9)
-OWN_TO_MATE_AFTER = {4: (10,), 7: (11,)}
+OWN_TO_MATE = (2, 3, 4, 5, 6, 7, 8, 9, 10)
+OWN_TO_MATE_AFTER = {6: (11,), 8: (12,), 5: (13,)}
 OWN_TO_OTHER = (0, 1)
-OWN_TO_OTHER_AFTER = {1: (2, 3), 3: (4, 5, 6), 6: (7,), 7: (8, 9, 10), 10: (11,)}
-EDGE_SENDS = ((1, 2), (1, 3), (0, 2), (0, 3), (1, 4), (1, 5), (1, 6), (1, 7), (0, 4), (0, 5), (0, 6), (0, 7), (1, 8), (1, 9), (1, 10), (1, 11), (0, 8), (0, 9), (0, 10), (0, 11))
+OWN_TO_OTHER_AFTER = {1: (2, 3), 3: (4, 5), 4: (6,), 6: (7,), 7: (8, 9), 8: (10,), 10: (11,), 11: (12, 13)}
+EDGE_SENDS = ((1, 2), (1, 3), (0, 2), (0, 3), (1, 4), (1, 5), (1, 6), (1, 7), (0, 4), (0, 5), (0, 6), (0, 7), (1, 8), (1, 9), (1, 10), (1, 11), (1, 12), (1, 13), (0, 8), (0, 9), (0, 10), (0, 11), (0, 12), (0, 13))
 DOWN_ORDER = ((0, 0), (0, 1), None, (1, 0), (1, 1), (0, 2), (1, 2), (0, 3), (1, 3), (0, 4), (1, 4), (0, 5), (1, 5), (0, 6), (1, 6), (0, 7), (1, 7))
 LAG = 8
 EDGE_SERVES = (
-    (2, 3, 4, 5, 6, 7, 8, 9, 14, 15),
-    (),
-    (),
-    (26,),
+    (2, 3, 4, 5, 6, 7, 8, 9, 10, 16, 17),
+    (),
+    (),
+    (30,),
+    (),
+    (31,),
+    (),
+    (),
+    (),
+    (18,),
+    (),
+    (),
+    (),
+    (19,),
+    (),
+    (),
+    (),
+    (),
+    (),
+    (32,),
+    (),
+    (),
+    (),
+    (20,),
+    (),
+    (),
+    (),
+    (33,),
+    (13,),
+    (),
+    (34,),
+    (11,),
+    (21,),
+    (),
+    (),
+    (),
+    (35, 22, 23),
+    (),
+    (),
+    (),
+    (),
+    (),
+    (),
+    (),
+    (),
+    (),
+    (),
+    (36, 12),
+    (),
+    (),
+    (),
+    (),
+    (),
+    (24,),
+    (),
+    (),
+    (),
+    (),
+    (),
+    (37,),
+    (),
+    (),
+    (38,),
+    (25, 39, 26),
+    (),
     (),
     (27,),
     (),
     (),
     (),
-    (16,),
-    (),
-    (),
-    (),
-    (17,),
-    (),
-    (),
-    (),
-    (),
-    (),
-    (18,),
-    (),
-    (),
-    (),
-    (28,),
-    (),
-    (),
-    (),
-    (10,),
-    (),
-    (29,),
-    (),
-    (30,),
-    (19,),
-    (),
-    (),
-    (),
-    (31, 11, 20),
-    (),
-    (),
-    (),
-    (),
-    (),
-    (),
-    (),
-    (),
-    (),
-    (),
-    (21,),
-    (),
-    (),
-    (),
-    (),
-    (),
-    (22,),
-    (),
-    (),
-    (),
-    (),
-    (),
-    (32,),
-    (),
-    (),
-    (),
-    (33, 34, 23),
-    (),
-    (),
-    (),
-    (),
-    (),
-    (),
-    (),
-    (35,),
-    (),
-    (),
+    (),
+    (40,),
+    (),
+    (41,),
     (),
     (),
     (),
@@ -308,10 +309,10 @@
     (),
     (),
     (),
-    (0, 12, 1, 13),
-    (24, 25),
-    (14,),
-    (15,),
+    (0, 14, 1, 15),
+    (28, 29),
+    (16,),
+    (17,),
     (),
     (),
     (),
@@ -319,74 +320,74 @@
     (3,),
     (),
     (),
+    (30,),
+    (),
+    (),
+    (31,),
+    (),
+    (),
+    (18, 4),
+    (),
+    (),
+    (19, 5),
+    (),
+    (),
+    (),
+    (),
+    (),
+    (32,),
+    (),
+    (6,),
+    (),
+    (),
+    (20,),
+    (),
+    (),
+    (7,),
+    (),
+    (),
+    (33,),
+    (),
+    (34,),
+    (),
+    (21,),
+    (),
+    (35,),
+    (22, 8),
+    (),
+    (),
+    (),
+    (),
+    (23,),
+    (9,),
+    (),
+    (),
+    (),
+    (),
+    (10,),
+    (36, 11),
+    (24, 12),
+    (13,),
+    (37, 38),
+    (),
+    (),
+    (25,),
+    (),
+    (),
+    (),
+    (),
+    (),
+    (39,),
+    (),
+    (),
     (26,),
     (),
     (),
-    (27,),
-    (),
-    (),
-    (16, 4),
-    (),
-    (),
-    (17, 5),
-    (),
-    (),
-    (),
-    (),
-    (),
-    (18,),
-    (),
-    (6,),
-    (),
-    (),
-    (28,),
-    (),
-    (),
-    (7,),
-    (),
-    (),
-    (29,),
-    (),
-    (30,),
-    (),
-    (19,),
-    (),
-    (31,),
-    (20, 8),
-    (),
-    (),
-    (),
-    (21,),
-    (),
-    (9,),
-    (),
-    (),
-    (),
-    (),
-    (),
-    (22, 10),
-    (),
-    (32, 11),
-    (33,),
-    (),
-    (),
-    (),
-    (),
-    (),
-    (),
-    (),
-    (),
-    (34,),
-    (),
-    (),
-    (),
-    (),
-    (),
-    (23,),
-    (),
-    (),
-    (),
-    (35,),
+    (27, 40),
+    (),
+    (),
+    (),
+    (41,),
     (),
     (),
     (),
@@ -417,10 +418,10 @@
 
 
 def layer_kernel(
-    names, tokens_hbm, first_ref, in_hbm, in_scale_ref, taps_ref, rate_ref, recall_hbm, admit_hbm,
-    out_hbm, out_scale_ref, second_ref, up_hbm, up_scale_ref, down_hbm, down_scale_ref,
+    names, tokens_hbm, first_hbm, in_hbm, in_scale_hbm, taps_hbm, rate_hbm, recall_hbm, admit_hbm,
+    out_hbm, out_scale_hbm, second_hbm, up_hbm, up_scale_hbm, down_hbm, down_scale_hbm,
     result_ref,
-    tokens, in_own, out_own, up_own, down_own, recall_ref, admit_ref,
+    first_ref, in_scale_ref, taps_ref, rate_ref, second_ref, up_scale_ref, tokens, in_own, out_own, up_own, down_own, recall_ref, admit_ref,
     in_all, out_all, up_all, down_all, scales_all, normed, guest, before, second_normed, padded, decay, drive, prefix,
     mixed, active, parts, near_parts, pairs, far_pairs, middle, load, send, recv,
 ):
@@ -438,73 +439,115 @@
     core = lax.rem(rank, 2)
     near = rank + 1 - 2 * core
     far = lax.rem(rank + 2, 4)
-    sends, recvs = [0], [0]
-
-    def fresh(counter):
-        counter[0] += 1
-        return counter[0] - 1
-
-    def copy(src, dst, axis, peer, into=None):
-        index = fresh(recvs) if into is None else into
+    recvs, groups = [0], {}
+
+    def fresh():
+        recvs[0] += 1
+        return recvs[0] - 1
+
+    def whole_copy(src, dst, axis, peer, group, into):
         return pltpu.make_async_remote_copy(
-            src_ref=src, dst_ref=dst, send_sem=send.at[fresh(sends)], recv_sem=recv.at[index],
+            src_ref=src, dst_ref=dst, send_sem=send.at[groups.setdefault(group, len(groups))], recv_sem=recv.at[into],
             device_id={axis: peer}, device_id_type=MESH,
         )
 
-    common_sent, edge_sent, inner_sent = [], [], []
+    def bytes_of(ref):
+        return math.prod(ref.shape) * jnp.dtype(ref.dtype).itemsize
+
+    def waiter(size, group, into):
+        count = size // bytes_of(up_all.at[0])
+        return whole_copy(up_all.at[0:count, :], up_all.at[0:count, :], tp_name, near, group, into)
+
+    class copy:
+        def __init__(self, src, dst, axis, peer, group, into=None):
+            self.into = fresh() if into is None else into
+            self.group, self.size = group, bytes_of(src)
+            self.one = whole_copy(src, dst, axis, peer, group, self.into)
+            self.start, self.wait_recv, self.wait_send = self.one.start, self.one.wait_recv, self.one.wait_send
+
+    common_sent, edge_sent, inner_sent = {}, {}, {}
 
     def start(one, sent=common_sent):
         one.start()
-        sent.append(one)
+        sent.setdefault(one.group, []).append(one)
+
+    def drain(sent):
+        for group, copies in sent.items():
+            if len(copies) == 1:
+                copies[0].wait_send()
+            else:
+                waiter(sum(one.size for one in copies), group, copies[0].into).wait_send()
+
+    def wait_all(copies):
+        waiter(sum(one.size for one in copies), copies[0].group, copies[0].into).wait_recv()
+
+    barrier = pltpu.get_barrier_semaphore()
+    greeted = [(rep_name, 1 - replica)]
+    greeted += [(fs_name, mate), (tp_name, near), (tp_name, far)]
+
+    def greet(axis, peer):
+        pl.semaphore_signal(barrier, inc=1, device_id={axis: peer}, device_id_type=MESH)
+
+    for axis, peer in greeted:
+        greet(axis, peer)
+    pl.when(inner == 1)(lambda: greet(fs_name, other))
 
     loads = [
         pltpu.make_async_copy(src, dst, load.at[i])
         for i, (src, dst) in enumerate((
-            (in_hbm, in_own), (tokens_hbm, tokens), (out_hbm, out_own), (up_hbm, up_own), (down_hbm, down_own),
-            (recall_hbm, recall_ref), (admit_hbm, admit_ref),
+            (in_hbm, in_own), (out_hbm, out_own), (first_hbm, first_ref), (tokens_hbm, tokens), (up_hbm, up_own),
+            (down_hbm, down_own), (out_scale_hbm, scales_all.at[place, 0:1, :]), (down_scale_hbm, scales_all.at[place, 1:2, :]),
+            (in_scale_hbm, in_scale_ref), (taps_hbm, taps_ref), (rate_hbm, rate_ref), (second_hbm, second_ref),
+            (up_scale_hbm, up_scale_ref), (recall_hbm, recall_ref), (admit_hbm, admit_ref),
         ))
     ]
     for one in loads:
         one.start()
-    load_in, load_tokens, load_out, load_up, load_down, load_recall, load_admit = loads
-
-    barrier = pltpu.get_barrier_semaphore()
-    greeted = [(rep_name, 1 - replica)]
-    greeted += [(fs_name, lax.rem(place + k, fs)) for k in range(1, fs)]
-    greeted += [(tp_name, near), (tp_name, far)]
-    for axis, peer in greeted:
-        pl.semaphore_signal(barrier, inc=1, device_id={axis: peer}, device_id_type=MESH)
+    load_in, load_out, load_first, load_tokens, load_up, load_down = loads[:6]
+    load_scales, load_rest = loads[6:8], loads[8:]
 
     own_rows = pl.ds(pl.multiple_of(place * block, block), block)
     load_in.wait()
     in_all[own_rows, :] = in_own[...].astype(jnp.bfloat16)
-    scales_all[place, 0:1, :] = out_scale_ref[...]
-    scales_all[place, 1:2, :] = down_scale_ref[...]
+    load_out.wait()
+    out_all[own_rows, :] = out_own[...].astype(jnp.bfloat16)
 
     wide = up_all.shape[1] // 2
 
     def view(owner, unit, side):
-        def rows(step):
-            return pl.ds(pl.multiple_of(owner * block + side * half + step * quarter, quarter), quarter)
+        def rows(first, count):
+            return pl.ds(pl.multiple_of(owner * block + side * half + first, count), count)
+
+        def columns(part):
+            return slice(part * wide, (part + 1) * wide)
 
         if unit < 4:
-            return (in_all, out_all)[unit // 2].at[rows(unit % 2), :]
+            return (in_all, out_all)[unit // 2].at[rows(unit % 2 * quarter, quarter), :]
         if unit < 8:
-            return up_all.at[rows(unit % 2), (unit - 4) // 2 * wide : ((unit - 4) // 2 + 1) * wide]
-        return down_all.at[rows((unit - 8) // 2), unit % 2 * wide : (unit % 2 + 1) * wide]
+            return up_all.at[rows(unit % 2 * quarter, quarter), columns((unit - 4) // 2)]
+        if unit < 10:
+            return down_all.at[rows(0, quarter), columns(unit - 8)]
+        return down_all.at[rows(quarter + (unit - 10) % 2 * (quarter // 2), quarter // 2), columns((unit - 10) // 2)]
 
     to_mate, extra, to_other, pass_mate, pass_other, pass_last, swaps = [], [], [], [], [], [], []
+    bundles = [(0, 1), (2, 3), (4, 5), (6, 7), (8, 9), tuple(range(10, UNITS))]
+    landings = {}
+    for bundle in bundles:
+        shared = [fresh() for _ in range(3 if bundle[0] >= 8 else 1)] * (1 if bundle[0] >= 8 else 3)
+        for unit in bundle:
+            landings[unit] = shared
     for unit in range(UNITS):
-        into = [fresh(recvs) for _ in range(6)]
+        into = [fresh() for _ in range(3)]
         own, first, second, third = (view(owner, unit, replica) for owner in (place,) + slots)
         rest = view(place, unit, 1 - replica)
-        to_mate.append(copy(own, own, fs_name, mate, into[0]))
-        extra.append(copy(rest, rest, fs_name, mate, into[3]))
-        to_other.append(copy(own, own, fs_name, other, into[1]))
-        pass_mate.append(copy(first, first, fs_name, other, into[2]))
-        pass_other.append(copy(second, second, fs_name, mate, into[1]))
-        pass_last.append(copy(third, third, fs_name, mate, into[2]))
-        swaps.append([copy(part, part, rep_name, 1 - replica, into[3 + j]) for j, part in enumerate((first, second, third))])
+        land = landings[unit]
+        to_mate.append(copy(own, own, fs_name, mate, "to_mate", into[0]))
+        extra.append(copy(rest, rest, fs_name, mate, "extra", land[0]) if unit >= SPLIT else None)
+        to_other.append(copy(own, own, fs_name, other, "to_other", into[1]))
+        pass_mate.append(copy(first, first, fs_name, other, "pass_mate", into[2]))
+        pass_other.append(copy(second, second, fs_name, mate, "pass_other", into[1]) if unit >= SPLIT else None)
+        pass_last.append(copy(third, third, fs_name, mate, "pass_last", into[2]))
+        swaps.append([copy(part, part, rep_name, 1 - replica, f"swap{j}", land[j]) for j, part in enumerate((first, second, third))])
     arrivals = (to_mate, to_other, pass_last)
 
     def serve_edge(codes):
@@ -547,9 +590,7 @@
             pl.when(inner == 1)(lambda: serve_inner(inner_codes))
 
     def landed(units, taken=(0, 1, 2)):
-        for unit in units:
-            for slot in taken:
-                swaps[unit][slot].wait_recv()
+        wait_all([swaps[unit][slot] for unit in units for slot in taken])
 
     piece = 32
     pieces = length // 4 // piece
@@ -558,17 +599,19 @@
         return pl.ds(pl.multiple_of(owner * (length // 4) + i * piece, piece), piece)
 
     tok, tok_far, tok_near, tok_onward = [], [], [], []
+    guest_near = fresh()
     for i in range(pieces):
         mine, theirs = guest_rows(rank, i), guest_rows(far, i)
-        tok.append(copy(normed.at[mine, :], guest.at[mine, :], fs_name, mate))
-        tok_far.append(copy(guest.at[mine, :], guest.at[mine, :], tp_name, far))
-        tok_near.append(copy(guest.at[mine, :], guest.at[mine, :], tp_name, near))
-        tok_onward.append(copy(guest.at[theirs, :], guest.at[theirs, :], tp_name, near))
+        tok.append(copy(normed.at[mine, :], guest.at[mine, :], fs_name, mate, "guest"))
+        tok_far.append(copy(guest.at[mine, :], guest.at[mine, :], tp_name, far, "guest"))
+        tok_near.append(copy(guest.at[mine, :], guest.at[mine, :], tp_name, near, "guest", guest_near))
+        tok_onward.append(copy(guest.at[theirs, :], guest.at[theirs, :], tp_name, near, "guest", guest_near))
     step = 256
     tiles = [slice(i * step, (i + 1) * step) for i in range(in_all.shape[1] // step)]
-    given_before = [copy(before.at[:, at], before.at[:, at], fs_name, mate) for at in tiles]
-
-    pl.semaphore_wait(barrier, len(greeted))
+    given_before = [copy(before.at[:, at], before.at[:, at], fs_name, mate, "guest") for at in tiles]
+
+    pl.when(inner == 0)(lambda: pl.semaphore_wait(barrier, len(greeted)))
+    pl.when(inner == 1)(lambda: pl.semaphore_wait(barrier, len(greeted) + 1))
 
     @pl.when(inner == 0)
     def _():
@@ -579,16 +622,14 @@
     def _():
         for unit in OWN_TO_OTHER:
             start(to_other[unit], inner_sent)
-
-    scale_copies = [
-        copy(scales_all.at[place], scales_all.at[place], fs_name, lax.rem(place + k, fs)) for k in range(1, fs)
-    ]
-    for one in scale_copies:
-        start(one)
+        for unit in OWN_TO_MATE:
+            if unit < 4:
+                start(to_mate[unit], inner_sent)
 
     def norm_rows(at):
         normed[at, :] = normalize(tokens[at, :].astype(jnp.float32), first_ref[...]).astype(jnp.bfloat16)
 
+    load_first.wait()
     load_tokens.wait()
 
     @pl.when(inner == 0)
@@ -597,21 +638,30 @@
             norm_rows(guest_rows(rank, i))
             start(tok[i], edge_sent)
 
-    load_out.wait()
-    out_all[own_rows, :] = out_own[...].astype(jnp.bfloat16)
-
-    @pl.when(inner == 1)
-    def _():
-        for unit in OWN_TO_MATE:
-            if unit < 4:
-                start(to_mate[unit], inner_sent)
-
     load_up.wait()
     up_all[own_rows, :] = up_own[...].astype(jnp.bfloat16)
     load_down.wait()
     down_all[own_rows, :] = down_own[...].astype(jnp.bfloat16)
-    load_recall.wait()
-    load_admit.wait()
+    for one in load_scales:
+        one.wait()
+    into = [fresh() for _ in range(3)]
+    own, first, second, third = (scales_all.at[owner] for owner in (place,) + slots)
+    scale_in = [
+        copy(own, own, fs_name, mate, "scale0", into[0]), copy(own, own, fs_name, other, "scale1", into[1]),
+        copy(third, third, fs_name, mate, "scale2", into[2]),
+    ]
+    scale_out = [
+        copy(first, first, fs_name, other, "scale3", into[2]), copy(second, second, fs_name, mate, "scale4", into[1]), scale_in[2],
+    ]
+    start(scale_in[0])
+    pl.when(inner == 1)(lambda: start(scale_in[1], inner_sent))
+
+    def pass_scales(slot):
+        scale_in[slot].wait_recv()
+        start(scale_out[slot], inner_sent)
+
+    for one in load_rest:
+        one.wait()
     edge = jnp.zeros((PAD, padded.shape[1]), jnp.float32)
     padded[pl.ds(0, PAD), :] = edge
     padded[pl.ds(PAD + length, PAD), :] = edge
@@ -644,14 +694,15 @@
             tok[i].wait_recv()
             start(tok_far[i], inner_sent)
             start(tok_near[i], inner_sent)
+        pass_scales(0)
+        pass_scales(1)
         for i in range(pieces):
             serve_inner(inner_next())
             tok_far[i].wait_recv()
             start(tok_onward[i], inner_sent)
         serve_inner(inner_next())
         landed(range(SPLIT))
-        for one in tok_near + tok_onward:
-            one.wait_recv()
+        wait_all(tok_near + tok_onward)
 
         def project_in(values, at):
             product = jnp.dot(values[...], in_all[:, at], preferred_element_type=jnp.float32)
@@ -661,6 +712,7 @@
             before[:, at] = project_in(guest, at)
             start(one, inner_sent)
             serve_inner(inner_next())
+        pass_scales(2)
         for at in tiles:
             padded[pl.ds(PAD, length), at] = project_in(normed, at).astype(jnp.float32)
             serve_inner(inner_next())
@@ -670,8 +722,12 @@
 
     serve()
     landed((2, 3))
-    for one in scale_copies:
-        one.wait_recv()
+
+    @pl.when(inner == 0)
+    def _():
+        for one in scale_in:
+            one.wait_recv()
+
     chunks = model // step
     rows = length // 2
     batch = rows // 2
@@ -684,10 +740,10 @@
     def factor(owner, which, at):
         return scales_all[owner, which : which + 1, at].astype(jnp.bfloat16).astype(jnp.float32)
 
-    to_near = [copy(parts.at[0, k, given, :], near_parts.at[0, k], tp_name, near) for k in range(chunks)]
+    to_near = [copy(parts.at[0, k, given, :], near_parts.at[0, k], tp_name, near, "reduce") for k in range(chunks)]
     to_far = [
         [
-            [copy(pairs.at[stage, k, of_batch(h), :], far_pairs.at[stage, k, of_batch(h), :], tp_name, far) for k in range(chunks)]
+            [copy(pairs.at[stage, k, of_batch(h), :], far_pairs.at[stage, k, of_batch(h), :], tp_name, far, "reduce") for k in range(chunks)]
             for h in range(2)
         ]
         for stage in range(2)
@@ -726,7 +782,7 @@
         inverse = lax.rsqrt(squares * (1.0 / model) + EPSILON)
         at = pl.ds(pl.multiple_of(h * rows + core * batch, batch), batch)
         second_normed[at, :] = (middle[of_batch(h), :] * inverse * second_ref[...]).astype(jnp.bfloat16)
-        spreads.append(copy(second_normed.at[at, :], second_normed.at[at, :], tp_name, near))
+        spreads.append(copy(second_normed.at[at, :], second_normed.at[at, :], tp_name, near, "spread"))
         start(spreads[h])
 
     def up_rows(h):
@@ -750,7 +806,7 @@
 
     owners = [(place, 0, None), (place, 1, None)] + [(slots[j], q, j) for q in range(2) for j in range(3)]
     turns = [turn for turn in DOWN_ORDER if turn is not None]
-    down_near, finals = [], []
+    down_near, finals, final = [], [], fresh()
 
     def pair_down(n):
         h, k = turns[n]
@@ -772,7 +828,7 @@
             at = pl.ds(pl.multiple_of(owner * block + s * half + q * quarter, quarter), quarter)
             value = middle[of_batch(h), at] + factor(owner, 1, inside) * total[:, s * quarter : (s + 1) * quarter]
             result_ref[at_rows, at] = value.astype(jnp.bfloat16)
-            finals.append(copy(result_ref.at[at_rows, at], result_ref.at[at_rows, at], tp_name, near))
+            finals.append(copy(result_ref.at[at_rows, at], result_ref.at[at_rows, at], tp_name, near, "spread", final))
             start(finals[-1])
 
     n = 0
@@ -784,14 +840,14 @@
         owner, q, j = owners[k]
         if j is not None and h == 0:
             serve()
-            landed((8 + 2 * q, 9 + 2 * q), (j,))
+            landed((range(8, 10), range(10, UNITS))[q], (j,))
         matrix = [
             down_all[pl.ds(pl.multiple_of(owner * block + s * half + q * quarter, quarter), quarter), :] for s in range(2)
         ]
         product = contract_last(active[h * rows : (h + 1) * rows, :], jnp.concatenate(matrix, axis=0))
         parts[1, k, h * rows : (h + 1) * rows, :] = product.astype(jnp.bfloat16)
         away = pl.ds(pl.multiple_of(h * rows + (1 - core) * batch, batch), batch)
-        down_near.append(copy(parts.at[1, k, away, :], near_parts.at[1, k, of_batch(h), :], tp_name, near))
+        down_near.append(copy(parts.at[1, k, away, :], near_parts.at[1, k, of_batch(h), :], tp_name, near, "reduce"))
         start(down_near[n])
         if n >= 1:
             pair_down(n - 1)
@@ -802,20 +858,10 @@
     for m in range(n - LAG, n):
         finish(m)
     serve()
-    for one in finals:
-        one.wait_recv()
-    for one in common_sent:
-        one.wait_send()
-
-    @pl.when(inner == 0)
-    def _():
-        for one in edge_sent:
-            one.wait_send()
-
-    @pl.when(inner == 1)
-    def _():
-        for one in inner_sent:
-            one.wait_send()
+    wait_all(finals)
+    drain(common_sent)
+    pl.when(inner == 0)(lambda: drain(edge_sent))
+    pl.when(inner == 1)(lambda: drain(inner_sent))
 
 
 def fused_body(
@@ -833,13 +879,19 @@
     rows = pltpu.VMEM((length, model), jnp.bfloat16)
     channels = pltpu.VMEM((length, width), jnp.bfloat16)
     vmem, hbm = pl.BlockSpec(memory_space=pltpu.VMEM), pl.BlockSpec(memory_space=pl.ANY)
-    count = UNITS * 7 + 3 + 16 + 2 + 9 * (model // step) + 2 + 4 * (model // step)
+    arrived = UNITS * 3 + 27 + 7 * (model // step)
     result = pl.pallas_call(
         functools.partial(layer_kernel, ("rep", "fs", "tp")),
         out_shape=pltpu.VMEM((length, model), jnp.bfloat16),
-        in_specs=[hbm, vmem, hbm, vmem, vmem, vmem, hbm, hbm, hbm, vmem, vmem, hbm, vmem, hbm, vmem],
+        in_specs=[hbm] * 15,
         out_specs=vmem,
         scratch_shapes=[
+            pltpu.VMEM((1, model), jnp.float32),
+            pltpu.VMEM((1, width), jnp.float32),
+            pltpu.VMEM(conv_taps.shape, jnp.float32),
+            pltpu.VMEM(decay_rate.shape, jnp.float32),
+            pltpu.VMEM((1, model), jnp.float32),
+            pltpu.VMEM((1, hidden), jnp.float32),
             rows,
             pltpu.VMEM((block, width), jnp.float32),
             pltpu.VMEM((block, width), jnp.float32),
@@ -859,9 +911,9 @@
             pltpu.VMEM((2, model // step, length, step), jnp.bfloat16),
             pieces, pieces, pieces,
             pltpu.VMEM((length // 2, model), jnp.float32),
-            pltpu.SemaphoreType.DMA((7,)),
-            pltpu.SemaphoreType.DMA((count + 3 * UNITS,)),
-            pltpu.SemaphoreType.DMA((count,)),
+            pltpu.SemaphoreType.DMA((15,)),
+            pltpu.SemaphoreType.DMA((17,)),
+            pltpu.SemaphoreType.DMA((arrived,)),
         ],
         compiler_params=pltpu.CompilerParams(
             collective_id=0, has_side_effects=True, vmem_limit_bytes=59 * 2**20

time: 123 us -> 119 us (0.967)
  Pallas kernels: 122 us -> 117 us
    pallas_call x1, Pallas kernels: 122 us -> 117 us  [fused_body(): pl.pallas_call(functools.partial(layer_kernel, ('rep', 'fs', 'tp')), out_...]
where the time goes in v3:
time: 119 us
  Pallas kernels  117 us (98%)
  local copies, waits for them, and re-layouts  1.32 us (1%)
    pallas_call x1, Pallas kernels, fused_body(): pl.pallas_call(functools.partial(layer_kernel, ('rep', 'fs', 'tp')), out_...  117 us

profile of v3, /device:TPU:0, one launch (start us, length us, event | category | flops | bytes accessed | tf_op | source)
XLA Modules:
  0.0 118.6 jit_solution(12006096111784480025)
XLA Ops:
  0.0 117.3 %layer.1 = bf16[512,2048]{1,0:T(8,128)(2,1)S(1)} custom-call(bf16[512,2048]{1,0:T(8,128)(2,1)} %bitcast.9, f32[1,2048]{1,0:T(1,128)} %bitcast.10, f32[512,512]{1,0:T(8,128)} %in_hbm.1, f32[1,512]{1,0:T(1,128)} %bitcast.13, f32[4,512]{1,0:T(4,128)} %taps_hbm.1, f32[2,512]{1,0:T(2,128)} %rate_hbm.1, f32[2,2,256,256]{3,2,1,0:T(8,128)} %recall_hbm.1, ...), custom_call_target="tpu_custom_call" | custom-call | tf_op jit(solution)/shard_map/layer/pallas_call | solution.py:883
  117.3 1.3 %copy.17 = bf16[1,512,2048]{2,1,0:T(8,128)(2,1)} copy(bf16[1,512,2048]{2,1,0:T(8,128)(2,1)S(1)} %bitcast.8) | data formatting | bytes 4194304

commit v4 on v3

--- a/solution.py
+++ b/solution.py
@@ -200,94 +200,94 @@
     return result.reshape(tokens.shape)
 
 MESH = pl.DeviceIdType.MESH
-UNITS = 14
+UNITS = 20
 SPLIT = 2
-OWN_TO_MATE = (2, 3, 4, 5, 6, 7, 8, 9, 10)
-OWN_TO_MATE_AFTER = {6: (11,), 8: (12,), 5: (13,)}
-OWN_TO_OTHER = (0, 1)
-OWN_TO_OTHER_AFTER = {1: (2, 3), 3: (4, 5), 4: (6,), 6: (7,), 7: (8, 9), 8: (10,), 10: (11,), 11: (12, 13)}
-EDGE_SENDS = ((1, 2), (1, 3), (0, 2), (0, 3), (1, 4), (1, 5), (1, 6), (1, 7), (0, 4), (0, 5), (0, 6), (0, 7), (1, 8), (1, 9), (1, 10), (1, 11), (1, 12), (1, 13), (0, 8), (0, 9), (0, 10), (0, 11), (0, 12), (0, 13))
-DOWN_ORDER = ((0, 0), (0, 1), None, (1, 0), (1, 1), (0, 2), (1, 2), (0, 3), (1, 3), (0, 4), (1, 4), (0, 5), (1, 5), (0, 6), (1, 6), (0, 7), (1, 7))
-LAG = 8
+OWN_TO_MATE = (2, 3, 4, 5, 6, 7, 8, 9, 10, 11, 12, 13, 14)
+OWN_TO_MATE_AFTER = {8: (15,), 15: (16, 17), 16: (18, 19)}
+OWN_TO_OTHER = (0, 1, 2)
+OWN_TO_OTHER_AFTER = {1: (3, 4), 2: (5, 6), 3: (7,), 4: (8,), 5: (9,), 8: (10, 11, 12), 12: (13, 14, 15, 16), 15: (17,), 16: (18, 19)}
+EDGE_SENDS = ((1, 2), (1, 3), (0, 2), (0, 3), (1, 4), (1, 5), (1, 6), (1, 7), (1, 8), (1, 9), (1, 10), (1, 11), (0, 4), (0, 5), (0, 6), (0, 7), (0, 8), (0, 9), (0, 10), (0, 11), (1, 12), (1, 13), (1, 14), (1, 15), (1, 16), (1, 17), (1, 18), (1, 19), (0, 12), (0, 13), (0, 14), (0, 15), (0, 16), (0, 17), (0, 18), (0, 19))
+DOWN_ORDER = ((0, 0), (0, 1), (0, 2), (0, 3), None, (1, 0), (1, 1), (1, 2), (1, 3), (0, 4), (1, 4), (0, 5), (1, 5), (0, 6), (1, 6), (0, 7), (1, 7))
+LAG = 4
 EDGE_SERVES = (
-    (2, 3, 4, 5, 6, 7, 8, 9, 10, 16, 17),
-    (),
-    (),
+    (2, 3, 4, 5, 6, 7, 8, 9, 10, 11, 12, 13, 14, 22, 23, 24, 42),
+    (25,),
+    (),
+    (26,),
+    (),
+    (43,),
+    (),
+    (27,),
+    (),
+    (44,),
+    (),
+    (28,),
+    (),
+    (),
+    (),
+    (45,),
+    (),
+    (),
+    (),
+    (29,),
+    (),
+    (),
+    (46, 47),
+    (),
+    (),
+    (48,),
+    (15,),
     (30,),
-    (),
     (31,),
-    (),
+    (32,),
+    (49,),
+    (50,),
+    (51, 52),
+    (),
+    (),
+    (),
+    (33, 34),
+    (),
+    (35,),
+    (),
+    (),
+    (),
+    (),
+    (),
+    (36,),
+    (53,),
+    (54,),
+    (55, 16),
+    (),
+    (),
+    (),
+    (17,),
+    (),
+    (),
+    (),
+    (37,),
+    (),
+    (),
+    (),
+    (),
+    (),
+    (56,),
     (),
     (),
     (18,),
     (),
-    (),
-    (),
     (19,),
     (),
     (),
-    (),
-    (),
-    (),
-    (32,),
-    (),
-    (),
-    (),
-    (20,),
-    (),
-    (),
-    (),
-    (33,),
-    (13,),
-    (),
-    (34,),
-    (11,),
-    (21,),
-    (),
-    (),
-    (),
-    (35, 22, 23),
-    (),
-    (),
-    (),
-    (),
-    (),
-    (),
-    (),
-    (),
-    (),
-    (),
-    (36, 12),
-    (),
-    (),
-    (),
-    (),
-    (),
-    (24,),
-    (),
-    (),
-    (),
-    (),
-    (),
-    (37,),
-    (),
-    (),
     (38,),
-    (25, 39, 26),
-    (),
-    (),
-    (27,),
-    (),
-    (),
-    (),
-    (),
-    (40,),
-    (),
-    (41,),
-    (),
-    (),
-    (),
-    (),
+    (),
+    (39,),
+    (57,),
+    (),
+    (),
+    (58,),
+    (),
+    (59,),
     (),
     (),
     (),
@@ -309,69 +309,74 @@
     (),
     (),
     (),
-    (0, 14, 1, 15),
-    (28, 29),
+    (0, 20, 1, 21),
+    (22, 40),
+    (41,),
+    (23,),
+    (),
+    (),
+    (24,),
+    (2,),
+    (3, 42),
+    (),
+    (25,),
+    (),
+    (),
+    (26,),
+    (),
+    (4, 43),
+    (5,),
+    (27, 6),
+    (),
+    (7, 44),
+    (8,),
+    (28,),
+    (),
+    (9,),
+    (45,),
+    (),
+    (),
+    (10,),
+    (29,),
+    (),
+    (),
+    (11, 46),
+    (),
+    (),
+    (47, 48),
+    (),
+    (),
+    (30,),
+    (31,),
+    (32,),
+    (49,),
+    (50,),
+    (51,),
+    (12,),
+    (13, 14),
+    (),
+    (52,),
+    (),
+    (15, 33),
+    (),
     (16,),
-    (17,),
-    (),
-    (),
-    (),
-    (2,),
-    (3,),
-    (),
-    (),
-    (30,),
-    (),
-    (),
-    (31,),
-    (),
-    (),
-    (18, 4),
-    (),
-    (),
-    (19, 5),
-    (),
-    (),
-    (),
-    (),
-    (),
-    (32,),
-    (),
-    (6,),
-    (),
-    (),
-    (20,),
-    (),
-    (),
-    (7,),
-    (),
-    (),
-    (33,),
-    (),
-    (34,),
-    (),
-    (21,),
-    (),
-    (35,),
-    (22, 8),
-    (),
-    (),
-    (),
-    (),
-    (23,),
-    (9,),
-    (),
-    (),
-    (),
-    (),
-    (10,),
-    (36, 11),
-    (24, 12),
-    (13,),
-    (37, 38),
-    (),
-    (),
-    (25,),
+    (),
+    (),
+    (),
+    (),
+    (34, 17, 35),
+    (18, 36),
+    (19, 53),
+    (54,),
+    (55,),
+    (37,),
+    (),
+    (),
+    (56,),
+    (),
+    (),
+    (38,),
+    (),
     (),
     (),
     (),
@@ -380,17 +385,12 @@
     (39,),
     (),
     (),
-    (26,),
-    (),
-    (),
-    (27, 40),
-    (),
-    (),
-    (),
-    (41,),
-    (),
-    (),
-    (),
+    (57,),
+    (58,),
+    (),
+    (),
+    (),
+    (59,),
     (),
     (),
     (),
@@ -523,17 +523,16 @@
 
         if unit < 4:
             return (in_all, out_all)[unit // 2].at[rows(unit % 2 * quarter, quarter), :]
-        if unit < 8:
-            return up_all.at[rows(unit % 2 * quarter, quarter), columns((unit - 4) // 2)]
-        if unit < 10:
-            return down_all.at[rows(0, quarter), columns(unit - 8)]
-        return down_all.at[rows(quarter + (unit - 10) % 2 * (quarter // 2), quarter // 2), columns((unit - 10) // 2)]
+        eighth = quarter // 2
+        if unit < 12:
+            return up_all.at[rows((unit - 4) % 4 * eighth, eighth), columns((unit - 4) // 4)]
+        return down_all.at[rows((unit - 12) // 4 * quarter + unit % 2 * eighth, eighth), columns((unit - 12) % 4 // 2)]
 
     to_mate, extra, to_other, pass_mate, pass_other, pass_last, swaps = [], [], [], [], [], [], []
-    bundles = [(0, 1), (2, 3), (4, 5), (6, 7), (8, 9), tuple(range(10, UNITS))]
+    bundles = [(0, 1), (2, 3)] + [tuple(range(i, i + 4)) for i in range(4, UNITS, 4)]
     landings = {}
     for bundle in bundles:
-        shared = [fresh() for _ in range(3 if bundle[0] >= 8 else 1)] * (1 if bundle[0] >= 8 else 3)
+        shared = [fresh() for _ in range(3 if bundle[0] >= 12 else 1)] * (1 if bundle[0] >= 12 else 3)
         for unit in bundle:
             landings[unit] = shared
     for unit in range(UNITS):
@@ -792,7 +791,7 @@
         for part in range(2):
             serve()
             if h == 0:
-                landed((4 + 2 * part, 5 + 2 * part))
+                landed(bundles[2 + part])
             for i in range(part * (wide // step), (part + 1) * (wide // step)):
                 at = slice(i * step, (i + 1) * step)
                 raised = jnp.dot(second_normed[at_rows, :], up_all[:, at], preferred_element_type=jnp.float32)
@@ -840,7 +839,7 @@
         owner, q, j = owners[k]
         if j is not None and h == 0:
             serve()
-            landed((range(8, 10), range(10, UNITS))[q], (j,))
+            landed(bundles[4 + q], (j,))
         matrix = [
             down_all[pl.ds(pl.multiple_of(owner * block + s * half + q * quarter, quarter), quarter), :] for s in range(2)
         ]

time: 119 us -> 118 us (level)
  no operation moved by 1% of the time
where the time goes in v4:
time: 118 us
  Pallas kernels  117 us (99%)
  local copies, waits for them, and re-layouts  1.32 us (1%)
    pallas_call x1, Pallas kernels, fused_body(): pl.pallas_call(functools.partial(layer_kernel, ('rep', 'fs', 'tp')), out_...  117 us

profile of v4, /device:TPU:0, one launch (start us, length us, event | category | flops | bytes accessed | tf_op | source)
XLA Modules:
  0.0 118.0 jit_solution(3289449408856732211)
XLA Ops:
  0.0 116.6 %layer.1 = bf16[512,2048]{1,0:T(8,128)(2,1)S(1)} custom-call(bf16[512,2048]{1,0:T(8,128)(2,1)} %bitcast.9, f32[1,2048]{1,0:T(1,128)} %bitcast.10, f32[512,512]{1,0:T(8,128)} %in_hbm.1, f32[1,512]{1,0:T(1,128)} %bitcast.13, f32[4,512]{1,0:T(4,128)} %taps_hbm.1, f32[2,512]{1,0:T(2,128)} %rate_hbm.1, f32[2,2,256,256]{3,2,1,0:T(8,128)} %recall_hbm.1, ...), custom_call_target="tpu_custom_call" | custom-call | tf_op jit(solution)/shard_map/layer/pallas_call | solution.py:882
  116.7 1.3 %copy.17 = bf16[1,512,2048]{2,1,0:T(8,128)(2,1)} copy(bf16[1,512,2048]{2,1,0:T(8,128)(2,1)S(1)} %bitcast.8) | data formatting | bytes 4194304

commit v5 on v4

--- a/solution.py
+++ b/solution.py
@@ -200,197 +200,197 @@
     return result.reshape(tokens.shape)
 
 MESH = pl.DeviceIdType.MESH
-UNITS = 20
+UNITS = 22
 SPLIT = 2
-OWN_TO_MATE = (2, 3, 4, 5, 6, 7, 8, 9, 10, 11, 12, 13, 14)
-OWN_TO_MATE_AFTER = {8: (15,), 15: (16, 17), 16: (18, 19)}
-OWN_TO_OTHER = (0, 1, 2)
-OWN_TO_OTHER_AFTER = {1: (3, 4), 2: (5, 6), 3: (7,), 4: (8,), 5: (9,), 8: (10, 11, 12), 12: (13, 14, 15, 16), 15: (17,), 16: (18, 19)}
-EDGE_SENDS = ((1, 2), (1, 3), (0, 2), (0, 3), (1, 4), (1, 5), (1, 6), (1, 7), (1, 8), (1, 9), (1, 10), (1, 11), (0, 4), (0, 5), (0, 6), (0, 7), (0, 8), (0, 9), (0, 10), (0, 11), (1, 12), (1, 13), (1, 14), (1, 15), (1, 16), (1, 17), (1, 18), (1, 19), (0, 12), (0, 13), (0, 14), (0, 15), (0, 16), (0, 17), (0, 18), (0, 19))
-DOWN_ORDER = ((0, 0), (0, 1), (0, 2), (0, 3), None, (1, 0), (1, 1), (1, 2), (1, 3), (0, 4), (1, 4), (0, 5), (1, 5), (0, 6), (1, 6), (0, 7), (1, 7))
+OWN_TO_MATE = (2, 3, 4, 5, 6, 7, 8, 9, 10, 11, 12, 13, 14, 15, 16)
+OWN_TO_MATE_AFTER = {10: (17,), 17: (18, 19, 20, 21)}
+OWN_TO_OTHER = (0, 1)
+OWN_TO_OTHER_AFTER = {1: (2, 3, 4, 5), 5: (6, 7), 7: (8,), 8: (9, 10), 10: (11, 12, 13), 12: (14, 15), 14: (16,), 16: (17, 18, 19), 17: (20,), 18: (21,)}
+EDGE_SENDS = ((1, 2), (1, 3), (1, 4), (1, 5), (0, 2), (0, 3), (0, 4), (0, 5), (1, 6), (1, 7), (1, 8), (1, 9), (1, 10), (1, 11), (1, 12), (1, 13), (0, 6), (0, 7), (0, 8), (0, 9), (0, 10), (0, 11), (0, 12), (0, 13), (1, 14), (1, 15), (1, 16), (1, 17), (1, 18), (1, 19), (1, 20), (1, 21), (0, 14), (0, 15), (0, 16), (0, 17), (0, 18), (0, 19), (0, 20), (0, 21))
+DOWN_ORDER = ((0, 0), (0, 1), None, (1, 0), (1, 1), (0, 2), (1, 2), (0, 3), (1, 3), (0, 4), (1, 4), (0, 5), (1, 5), (0, 6), (1, 6), (0, 7), (1, 7))
 LAG = 4
 EDGE_SERVES = (
-    (2, 3, 4, 5, 6, 7, 8, 9, 10, 11, 12, 13, 14, 22, 23, 24, 42),
-    (25,),
-    (),
-    (26,),
-    (),
+    (2, 3, 4, 5, 6, 7, 8, 9, 10, 11, 12, 13, 14, 15, 16, 24, 25, 26, 27, 46, 47),
+    (48,),
+    (),
+    (49,),
+    (28,),
+    (29,),
+    (),
+    (50,),
+    (),
+    (51,),
+    (),
+    (30,),
+    (),
+    (),
+    (),
+    (),
+    (52,),
+    (),
+    (),
+    (31,),
+    (),
+    (),
+    (32, 53),
+    (),
+    (),
+    (54,),
+    (17,),
+    (33,),
+    (34,),
+    (35,),
+    (55,),
+    (56,),
+    (36,),
+    (),
+    (37,),
+    (),
+    (57, 58, 38, 59),
+    (),
+    (),
+    (),
+    (),
+    (),
+    (),
+    (),
+    (),
+    (),
+    (60, 39),
+    (40, 41),
+    (),
+    (),
+    (),
+    (),
+    (),
+    (),
+    (61,),
+    (),
+    (18,),
+    (),
+    (),
+    (),
+    (19,),
+    (),
+    (),
+    (),
+    (20,),
+    (),
+    (21,),
+    (),
+    (),
+    (42,),
+    (),
+    (62,),
     (43,),
     (),
-    (27,),
-    (),
-    (44,),
-    (),
+    (),
+    (),
+    (63,),
+    (64, 65),
+    (),
+    (),
+    (),
+    (),
+    (),
+    (),
+    (),
+    (),
+    (),
+    (),
+    (),
+    (),
+    (),
+    (),
+    (),
+)
+INNER_SERVES = (
+    (),
+    (),
+    (),
+    (),
+    (0, 22, 1, 23),
+    (44, 45),
+    (24,),
+    (25, 26),
+    (),
+    (),
+    (27, 2),
+    (3, 4, 46),
+    (5,),
+    (47,),
+    (),
+    (48,),
+    (),
+    (49,),
     (28,),
-    (),
-    (),
-    (),
-    (45,),
-    (),
-    (),
-    (),
     (29,),
-    (),
-    (),
-    (46, 47),
-    (),
-    (),
-    (48,),
-    (15,),
-    (30,),
-    (31,),
-    (32,),
-    (49,),
-    (50,),
-    (51, 52),
-    (),
-    (),
-    (),
-    (33, 34),
-    (),
-    (35,),
-    (),
-    (),
-    (),
-    (),
-    (),
-    (36,),
+    (6,),
+    (7,),
+    (),
+    (8,),
+    (50, 9),
+    (),
+    (),
+    (51, 10),
+    (),
+    (),
+    (),
+    (),
+    (30, 11),
+    (),
+    (),
+    (52, 12),
+    (),
+    (),
+    (31, 13, 32),
+    (),
+    (),
     (53,),
     (54,),
-    (55, 16),
-    (),
-    (),
-    (),
-    (17,),
-    (),
-    (),
-    (),
-    (37,),
-    (),
-    (),
-    (),
-    (),
-    (),
+    (33,),
+    (34,),
+    (35,),
+    (55,),
     (56,),
-    (),
-    (),
-    (18,),
-    (),
-    (19,),
-    (),
-    (),
-    (38,),
-    (),
-    (39,),
-    (57,),
-    (),
-    (),
-    (58,),
-    (),
-    (59,),
-    (),
-    (),
-    (),
-    (),
-    (),
-    (),
-    (),
-    (),
-    (),
-    (),
-    (),
-    (),
-    (),
-    (),
-    (),
-)
-INNER_SERVES = (
-    (),
-    (),
-    (),
-    (),
-    (0, 20, 1, 21),
-    (22, 40),
-    (41,),
-    (23,),
-    (),
-    (),
-    (24,),
-    (2,),
-    (3, 42),
-    (),
-    (25,),
-    (),
-    (),
-    (26,),
-    (),
-    (4, 43),
-    (5,),
-    (27, 6),
-    (),
-    (7, 44),
-    (8,),
-    (28,),
-    (),
-    (9,),
-    (45,),
-    (),
-    (),
-    (10,),
-    (29,),
-    (),
-    (),
-    (11, 46),
-    (),
-    (),
-    (47, 48),
-    (),
-    (),
-    (30,),
-    (31,),
-    (32,),
-    (49,),
-    (50,),
-    (51,),
-    (12,),
-    (13, 14),
-    (),
-    (52,),
-    (),
-    (15, 33),
-    (),
-    (16,),
-    (),
-    (),
-    (),
-    (),
-    (34, 17, 35),
-    (18, 36),
-    (19, 53),
-    (54,),
-    (55,),
-    (37,),
-    (),
-    (),
-    (56,),
-    (),
-    (),
-    (38,),
-    (),
-    (),
-    (),
-    (),
-    (),
-    (),
-    (39,),
-    (),
-    (),
-    (57,),
-    (58,),
-    (),
-    (),
-    (),
-    (59,),
+    (36, 14, 37, 15),
+    (),
+    (),
+    (),
+    (57, 16, 58, 17, 38, 18, 59, 19),
+    (),
+    (),
+    (),
+    (),
+    (),
+    (),
+    (),
+    (),
+    (60, 20),
+    (39, 21),
+    (40, 41),
+    (),
+    (),
+    (),
+    (),
+    (),
+    (61,),
+    (),
+    (),
+    (42,),
+    (),
+    (),
+    (),
+    (62,),
+    (43,),
+    (),
+    (),
+    (63,),
+    (),
+    (64,),
+    (),
+    (),
+    (65,),
     (),
     (),
     (),
@@ -521,18 +521,20 @@
         def columns(part):
             return slice(part * wide, (part + 1) * wide)
 
-        if unit < 4:
-            return (in_all, out_all)[unit // 2].at[rows(unit % 2 * quarter, quarter), :]
         eighth = quarter // 2
-        if unit < 12:
-            return up_all.at[rows((unit - 4) % 4 * eighth, eighth), columns((unit - 4) // 4)]
-        return down_all.at[rows((unit - 12) // 4 * quarter + unit % 2 * eighth, eighth), columns((unit - 12) % 4 // 2)]
+        if unit < 2:
+            return in_all.at[rows(unit * quarter, quarter), :]
+        if unit < 6:
+            return out_all.at[rows((unit - 2) * eighth, eighth), :]
+        if unit < 14:
+            return up_all.at[rows((unit - 6) % 4 * eighth, eighth), columns((unit - 6) // 4)]
+        return down_all.at[rows((unit - 14) // 4 * quarter + unit % 2 * eighth, eighth), columns((unit - 14) % 4 // 2)]
 
     to_mate, extra, to_other, pass_mate, pass_other, pass_last, swaps = [], [], [], [], [], [], []
-    bundles = [(0, 1), (2, 3)] + [tuple(range(i, i + 4)) for i in range(4, UNITS, 4)]
+    bundles = [(0, 1)] + [tuple(range(i, i + 4)) for i in range(2, UNITS, 4)]
     landings = {}
     for bundle in bundles:
-        shared = [fresh() for _ in range(3 if bundle[0] >= 12 else 1)] * (1 if bundle[0] >= 12 else 3)
+        shared = [fresh() for _ in range(3 if bundle[0] >= 14 else 1)] * (1 if bundle[0] >= 14 else 3)
         for unit in bundle:
             landings[unit] = shared
     for unit in range(UNITS):
@@ -622,7 +624,7 @@
         for unit in OWN_TO_OTHER:
             start(to_other[unit], inner_sent)
         for unit in OWN_TO_MATE:
-            if unit < 4:
+            if unit < 6:
                 start(to_mate[unit], inner_sent)
 
     def norm_rows(at):
@@ -677,7 +679,7 @@
     @pl.when(inner == 1)
     def _():
         for unit in OWN_TO_MATE:
-            if unit >= 4:
+            if unit >= 6:
                 start(to_mate[unit], inner_sent)
         tile = 64
         for i in range(4):
@@ -720,7 +722,7 @@
     scan_part(decay, drive, prefix, mixed, length, serve)
 
     serve()
-    landed((2, 3))
+    landed(bundles[1])
 
     @pl.when(inner == 0)
     def _():

time: 118 us -> 117 us (level)
  Pallas kernels: 117 us -> 115 us
where the time goes in v5:
time: 117 us
  Pallas kernels  115 us (98%)
  local copies, waits for them, and re-layouts  1.32 us (1%)
    pallas_call x1, Pallas kernels, fused_body(): pl.pallas_call(functools.partial(layer_kernel, ('rep', 'fs', 'tp')), out_...  115 us

profile of v5, /device:TPU:0, one launch (start us, length us, event | category | flops | bytes accessed | tf_op | source)
XLA Modules:
  0.0 116.8 jit_solution(5532596507995651130)
XLA Ops:
  0.0 115.5 %layer.1 = bf16[512,2048]{1,0:T(8,128)(2,1)S(1)} custom-call(bf16[512,2048]{1,0:T(8,128)(2,1)} %bitcast.9, f32[1,2048]{1,0:T(1,128)} %bitcast.10, f32[512,512]{1,0:T(8,128)} %in_hbm.1, f32[1,512]{1,0:T(1,128)} %bitcast.13, f32[4,512]{1,0:T(4,128)} %taps_hbm.1, f32[2,512]{1,0:T(2,128)} %rate_hbm.1, f32[2,2,256,256]{3,2,1,0:T(8,128)} %recall_hbm.1, ...), custom_call_target="tpu_custom_call" | custom-call | tf_op jit(solution)/shard_map/layer/pallas_call | solution.py:884
  115.5 1.3 %copy.17 = bf16[1,512,2048]{2,1,0:T(8,128)(2,1)} copy(bf16[1,512,2048]{2,1,0:T(8,128)(2,1)S(1)} %bitcast.8) | data formatting | bytes 4194304
